TPU v7x, 256 devices: a whole 4x4x8 slice. The times are simulated.
256 devices in a mesh: fs: 32 (over z, x), tp: 8 (over y, core).
Axes of the slice: x: 4, y: 4, z: 8, core: 2. Of those that a mesh axis runs over, the one named last changes fastest.
Arguments:
- later_rows: bfloat16 [32768, 2048], P(('fs', 'tp')), may hold values from -6 to 6
- earlier_rows: bfloat16 [32768, 2048], P(('fs', 'tp')), may hold values from -6 to 6
- cotangent: bfloat16 [32768, 2048], P(('fs', 'tp')), may hold values from -24 to 24
- up_weight: bfloat16 [2048, 4096], P('fs', 'tp'), may hold values from -0.125 to 0.125
- down_weight: bfloat16 [2048, 4096], P('fs', 'tp'), may hold values from -0.09375 to 0.09375
- up_total: float32 [2048, 4096], P('fs', 'tp'), may hold values from -6 to 6
- down_total: float32 [2048, 4096], P('fs', 'tp'), may hold values from -6 to 6
Outputs:
- later_out: bfloat16 [32768, 2048], P(('fs', 'tp'))
- earlier_grad: bfloat16 [32768, 2048], P(('fs', 'tp'))
- up_updated: float32 [2048, 4096], P('fs', 'tp')
- down_updated: float32 [2048, 4096], P('fs', 'tp')
All inputs are finite; a program needn't handle non-finite values.
Results may differ from a plain program's by a relative error of at most 0.015.
Values may be sent and summed in bfloat16 or wider, within the bound.
A program may use at most 128 MiB of HBM per device.

v0:
```python
import math

import jax
import jax.numpy as jnp
from jax import lax
from jax.sharding import Mesh
from jax.sharding import PartitionSpec as P

FS = ("fs_0", "fs_1")
FS_TP = ("fs_0", "fs_1", "tp")


def side_by_side(arrays, axis, dim, along):
    ends, at = ([], 0)
    for a in arrays[:-1]:
        at += a.shape[along]
        ends.append(at)
    both = jnp.concatenate(arrays, axis=along)
    return tuple(jnp.split(lax.all_gather(both, axis, axis=dim, tiled=True), ends, axis=along))


def in_blocks(x, dim, length):
    before, after = (x.shape[:dim], x.shape[dim + 1 :])
    return jnp.moveaxis(x.reshape(*before, length, -1, *after), dim, 0)


def sum_at_owner(x, axis, dim):
    length = lax.axis_size(axis)
    tiles = lax.all_to_all(in_blocks(x, dim, length), axis, 0, 0, tiled=True)
    return jnp.sum(tiles.astype(jnp.float32), axis=0)


def sum_by_axis(terms, axes):
    subtotal = terms.astype(jnp.bfloat16)
    for axis in axes:
        subtotal = lax.psum_scatter(subtotal, axis, scatter_dimension=0, tiled=True)
    return subtotal.astype(jnp.float32)


def contract_last(left, right):
    return lax.dot_general(
        left, right, (((1,), (1,)), ((), ())), preferred_element_type=jnp.float32
    )


def body(later_rows, earlier_rows, cotangent, up_weight, down_weight, up_total, down_total):
    rows_dev = later_rows.shape[0]
    total_rows = rows_dev * lax.axis_size(FS) * lax.axis_size("tp")
    factor = 1.0 / math.sqrt(total_rows)
    up_full, down_full = side_by_side((up_weight, down_weight), FS, 0, 1)

    def fetch():
        return (up_full, down_full)

    def to_owner(term):
        return sum_at_owner(term.astype(jnp.bfloat16), "tp", 0)

    def grad_owner(group, right):
        return sum_by_axis(
            lax.dot_general(
                group, right, (((0,), (0,)), ((), ())), preferred_element_type=jnp.float32
            ),
            FS,
        )

    up_whole, down_whole = fetch()
    group = lax.all_gather(later_rows, "tp", axis=0, tiled=True)
    relu_part = jnp.maximum(jnp.dot(group, up_whole, preferred_element_type=jnp.float32), 0.0)
    hidden = (relu_part * relu_part).astype(jnp.bfloat16)
    partial_value = contract_last(hidden, down_whole)
    later_out = to_owner(partial_value).astype(jnp.bfloat16)
    up_whole, down_whole = fetch()
    saved_group, cot_group = side_by_side((earlier_rows, cotangent), "tp", 0, 1)
    relu_part = jnp.maximum(jnp.dot(saved_group, up_whole, preferred_element_type=jnp.float32), 0.0)
    hidden = (relu_part * relu_part).astype(jnp.bfloat16)
    hidden_grad = jnp.dot(cot_group, down_whole, preferred_element_type=jnp.float32)
    pre_grad = (2.0 * relu_part * hidden_grad).astype(jnp.bfloat16)
    input_partial = contract_last(pre_grad, up_whole)
    earlier_grad = to_owner(input_partial).astype(jnp.bfloat16)
    down_updated = down_total + grad_owner(cot_group, hidden) * factor
    up_updated = up_total + grad_owner(saved_group, pre_grad) * factor
    earlier_grad, up_updated, down_updated = (earlier_grad, up_updated, down_updated)
    return (later_out, earlier_grad, up_updated, down_updated)


def solution(mesh):
    finer = Mesh(mesh.devices.reshape(8, 4, mesh.shape["tp"]), ("fs_0", "fs_1", "tp"))
    placed = (
        P(FS_TP, None),
        P(FS_TP, None),
        P(FS_TP, None),
        P(FS, "tp"),
        P(FS, "tp"),
        P(FS, "tp"),
        P(FS, "tp"),
    )
    return jax.shard_map(
        body,
        mesh=finer,
        in_specs=placed,
        out_specs=(P(FS_TP, None), P(FS_TP, None), P(FS, "tp"), P(FS, "tp")),
        check_vma=False,
    )
```

profile of v0, /device:TPU:1, one launch (start us, length us, event | category | flops | bytes accessed | tf_op | source)
XLA Modules:
  0.0 329.3 jit_solution(11753121503092980763)
XLA Ops:
  7.2 1.5 pad_maximum_fusion.1
  8.8 2.3 pad_maximum_fusion
  11.2 0.7 all-gather.6.cloned.1.call-update
  11.9 81.3 %all-gather.4.cloned.1.call-done = bf16[2048,1024]{1,0:T(8,128)(2,1)} async-done(((bf16[64,1024]{1,0:T(8,128)(2,1)}), bf16[2048,1024]{1,0:T(8,128)(2,1)}) %all-gather.4.cloned.1.call-update) | async-done | bytes 4194320 | tf_op jit(solution)/shard_map/all_gather | solution.py:19
  93.2 54.9 %all-gather.8.cloned.1.call-done = bf16[1024,4096]{1,0:T(8,128)(2,1)} async-done(((bf16[128,4096]{1,0:T(8,128)(2,1)}), bf16[1024,4096]{1,0:T(8,128)(2,1)}) %all-gather.8.cloned.1.call-update) | async-done | bytes 8388624 | tf_op jit(solution)/shard_map/all_gather | solution.py:19
  148.0 5.3 %fusion.6 = f32[1024,512]{1,0:T(8,128)S(1)} fusion(bf16[1024,4096]{1,0:T(8,128)(2,1)} %all-gather.8.cloned.1.call-done, bf16[2048,1024]{1,0:T(8,128)(2,1)} %all-gather.4.cloned.1.call-done), kind=kOutput, calls=%fused_computation.8 | convolution fusion | flops 2147483648 | bytes 8388608 | tf_op jit(solution)/shard_map/dot_general | solution.py:74
  153.4 3.7 %fusion.11 = bf16[2048,512]{1,0:T(8,128)(2,1)} fusion(bf16[1024,4096]{1,0:T(8,128)(2,1)S(1)} %copy-done.2, f32[1024,512]{1,0:T(8,128)S(1)} %fusion.6), kind=kOutput, calls=%fused_computation.11 | convolution fusion | flops 2150105088 | bytes 8388608 | tf_op jit(solution)/shard_map/dot_general | solution.py:60
  157.1 27.6 %all-gather.6.cloned.1.call-done = bf16[1024,2048]{1,0:T(8,128)(2,1)} async-done(((bf16[128,2048]{1,0:T(8,128)(2,1)}), bf16[1024,2048]{1,0:T(8,128)(2,1)}) %all-gather.6.cloned.1.call-update) | async-done | bytes 4194320 | tf_op jit(solution)/shard_map/all_gather | solution.py:67
  184.7 10.0 %convolution_convert_fusion.1 = bf16[1024,2048]{1,0:T(8,128)(2,1)} fusion(bf16[2048,1024]{1,0:T(8,128)(2,1)} %all-gather.4.cloned.1.call-done, bf16[1024,2048]{1,0:T(8,128)(2,1)} %all-gather.6.cloned.1.call-done), kind=kOutput, calls=%fused_computation.1 | convolution fusion | flops 4298637312 | bytes 12582912 | tf_op jit(solution)/shard_map/dot_general | solution.py:41
  194.7 4.7 %all-to-all-start = ((bf16[8,128,2048]{2,1,0:T(8,128)(2,1)}), bf16[8,128,2048]{2,1,0:T(8,128)(2,1)}, u32[]{:S(2)}, u32[]{:S(2)}) async-start(bf16[8,128,2048]{2,1,0:T(8,128)(2,1)} %bitcast.6), calls=%async_computation | async-start | bytes 8388608 | tf_op jit(solution)/shard_map/all_to_all | solution.py:29
  199.4 0.1 reduce-scatter.5.cloned.1.call-start
  199.5 5.2 %multiply_convert_fusion.1 = bf16[1024,512]{1,0:T(8,128)(2,1)S(1)} fusion(f32[1024,512]{1,0:T(8,128)S(1)} %fusion.6, bf16[2048,1024]{1,0:T(8,128)(2,1)} %all-gather.4.cloned.1.call-done, bf16[1024,4096]{1,0:T(8,128)(2,1)} %all-gather.8.cloned.1.call-done), kind=kOutput, calls=%fused_computation.13 | convolution fusion | flops 2149580800 | bytes 9437184 | tf_op jit(solution)/shard_map/dot_general | solution.py:76
  204.7 6.0 %fusion.8 = bf16[2048,512]{1,0:T(8,128)(2,1)} fusion(bf16[1024,512]{1,0:T(8,128)(2,1)S(1)} %multiply_convert_fusion.1, bf16[1024,4096]{1,0:T(8,128)(2,1)} %all-gather.8.cloned.1.call-done), kind=kOutput, calls=%fused_computation.10 | convolution fusion | flops 2148532224 | bytes 7340032 | tf_op jit(solution)/shard_map/dot_general | solution.py:60
  210.7 5.9 %convolution_convert_fusion = bf16[1024,2048]{1,0:T(8,128)(2,1)} fusion(bf16[1024,512]{1,0:T(8,128)(2,1)S(1)} %multiply_convert_fusion.1, bf16[2048,1024]{1,0:T(8,128)(2,1)} %all-gather.4.cloned.1.call-done), kind=kOutput, calls=%fused_computation | convolution fusion | flops 2149580800 | bytes 7340032 | tf_op jit(solution)/shard_map/dot_general | solution.py:41
  216.6 31.6 %all-to-all-done = bf16[8,128,2048]{2,1,0:T(8,128)(2,1)} async-done(((bf16[8,128,2048]{2,1,0:T(8,128)(2,1)}), bf16[8,128,2048]{2,1,0:T(8,128)(2,1)}, u32[]{:S(2)}, u32[]{:S(2)}) %all-to-all-start) | async-done | bytes 4194336 | tf_op jit(solution)/shard_map/all_to_all | solution.py:29
  248.2 5.4 %all-to-all-start.1 = ((bf16[8,128,2048]{2,1,0:T(8,128)(2,1)}), bf16[8,128,2048]{2,1,0:T(8,128)(2,1)}, u32[]{:S(2)}, u32[]{:S(2)}) async-start(bf16[8,128,2048]{2,1,0:T(8,128)(2,1)} %bitcast.5), calls=%async_computation.1 | async-start | bytes 8388608 | tf_op jit(solution)/shard_map/all_to_all | solution.py:29
  253.6 0.6 reduce-scatter.11.cloned.1.call-update
  254.2 14.7 %reduce-scatter.5.cloned.1.call-done = bf16[256,512]{1,0:T(8,128)(2,1)} async-done(((bf16[2048,512]{1,0:T(8,128)(2,1)}), bf16[256,512]{1,0:T(8,128)(2,1)}) %reduce-scatter.5.cloned.1.call-update) | async-done | bytes 262160 | tf_op jit(solution)/shard_map/reduce_scatter | solution.py:36
  269.0 3.9 %reduce_sum.24 = bf16[128,2048]{1,0:T(8,128)(2,1)} reduce(bf16[8,128,2048]{2,1,0:T(8,128)(2,1)} %all-to-all-done, bf16[]{:T(256)} %constant.3.clone.1), dimensions={0}, to_apply=%region_0.0 | reduce | flops 1835008 | bytes 4718594 | tf_op jit(solution)/shard_map/reduce_sum | solution.py:30
  272.9 29.6 %all-to-all-done.1 = bf16[8,128,2048]{2,1,0:T(8,128)(2,1)} async-done(((bf16[8,128,2048]{2,1,0:T(8,128)(2,1)}), bf16[8,128,2048]{2,1,0:T(8,128)(2,1)}, u32[]{:S(2)}, u32[]{:S(2)}) %all-to-all-start.1) | async-done | bytes 4194336 | tf_op jit(solution)/shard_map/all_to_all | solution.py:29
  302.4 3.8 %reduce_sum.25 = bf16[128,2048]{1,0:T(8,128)(2,1)} reduce(bf16[8,128,2048]{2,1,0:T(8,128)(2,1)} %all-to-all-done.1, bf16[]{:T(256)} %constant.3.clone.1), dimensions={0}, to_apply=%region_1.0 | reduce | flops 1835008 | bytes 4718594 | tf_op jit(solution)/shard_map/reduce_sum | solution.py:30
  306.3 1.5 multiply_add_fusion
  307.8 13.1 %reduce-scatter.7.cloned.1.call-done = bf16[64,512]{1,0:T(8,128)(2,1)} async-done(((bf16[256,512]{1,0:T(8,128)(2,1)}), bf16[64,512]{1,0:T(8,128)(2,1)}) %reduce-scatter.7.cloned.1.call-update) | async-done | bytes 65552 | tf_op jit(solution)/shard_map/reduce_scatter | solution.py:36
  320.9 1.5 multiply_add_fusion.1
  (19 shorter events, 0.3 us)
Async XLA Ops:
  7.2 86.0 %all-gather.4.cloned.1.call-start = ((), (), s32[]{:S(2)}) async-start(), calls=%async_computation.6 | async-start | bytes 4325376 | tf_op jit(solution)/shard_map/all_gather | solution.py:19
  8.8 139.3 %all-gather.8.cloned.1.call-start = ((), (), s32[]{:S(2)}) async-start(), calls=%async_computation.8 | async-start | bytes 9437184 | tf_op jit(solution)/shard_map/all_gather | solution.py:19
  11.1 173.6 %all-gather.6.cloned.1.call-start = ((), (), s32[]{:S(2)}) async-start(), calls=%async_computation.7 | async-start | bytes 4718592 | tf_op jit(solution)/shard_map/all_gather | solution.py:67
  11.9 241.8 %reduce-scatter.9.cloned.1.call-start = ((), (), s32[]{:S(2)}) async-start(), calls=%async_computation.11 | async-start | bytes 2359296 | tf_op jit(solution)/shard_map/reduce_scatter | solution.py:36
  148.0 5.3 %copy-start.2 = (bf16[1024,4096]{1,0:T(8,128)(2,1)S(1)}, bf16[1024,4096]{1,0:T(8,128)(2,1)}, u32[]{:S(2)}) copy-start(bf16[1024,4096]{1,0:T(8,128)(2,1)} %all-gather.8.cloned.1.call-done) | copy-start | bytes 25165828
  194.7 53.5 %all-to-all-start = ((bf16[8,128,2048]{2,1,0:T(8,128)(2,1)}), bf16[8,128,2048]{2,1,0:T(8,128)(2,1)}, u32[]{:S(2)}, u32[]{:S(2)}) async-start(bf16[8,128,2048]{2,1,0:T(8,128)(2,1)} %bitcast.6), calls=%async_computation | async-start | bytes 8388608 | tf_op jit(solution)/shard_map/all_to_all | solution.py:29
  199.4 69.5 %reduce-scatter.5.cloned.1.call-start = ((), (), s32[]{:S(2)}) async-start(), calls=%async_computation.9 | async-start | bytes 2359296 | tf_op jit(solution)/shard_map/reduce_scatter | solution.py:36
  248.2 54.2 %all-to-all-start.1 = ((bf16[8,128,2048]{2,1,0:T(8,128)(2,1)}), bf16[8,128,2048]{2,1,0:T(8,128)(2,1)}, u32[]{:S(2)}, u32[]{:S(2)}) async-start(bf16[8,128,2048]{2,1,0:T(8,128)(2,1)} %bitcast.5), calls=%async_computation.1 | async-start | bytes 8388608 | tf_op jit(solution)/shard_map/all_to_all | solution.py:29
  253.6 52.7 %reduce-scatter.11.cloned.1.call-start = ((), (), s32[]{:S(2)}) async-start(), calls=%async_computation.12 | async-start | bytes 327680 | tf_op jit(solution)/shard_map/reduce_scatter | solution.py:36
  254.2 66.7 %reduce-scatter.7.cloned.1.call-start = ((), (), s32[]{:S(2)}) async-start(), calls=%async_computation.10 | async-start | bytes 327680 | tf_op jit(solution)/shard_map/reduce_scatter | solution.py:36
  269.0 37.3 %copy-start = (f32[64,512]{1,0:T(8,128)S(1)}, f32[64,512]{1,0:T(8,128)}, u32[]{:S(2)}) copy-start(f32[64,512]{1,0:T(8,128)} %param.13) | copy-start | bytes 393220
  269.0 51.9 %copy-start.1 = (f32[64,512]{1,0:T(8,128)S(1)}, f32[64,512]{1,0:T(8,128)}, u32[]{:S(2)}) copy-start(f32[64,512]{1,0:T(8,128)} %param.12) | copy-start | bytes 393220
Sparse Core Ops, SparseCore 0:
  11.1 81.9 all-gather.3
  95.0 52.9 all-gather.7
  149.9 34.7 all-gather.5
  187.1 38.0 reduce-scatter.8
  227.6 41.3 reduce-scatter.4
  271.3 24.7 reduce-scatter.10
  298.6 22.2 reduce-scatter.6
where the time goes:
time: 331 us; the launch traced here: 329 us
  waiting for transfers between devices  254 us (77%)
  matrix products  36.1 us (11%)
  other arithmetic  14.6 us (4%)
  between operations  14.2 us (4%)
  starting transfers between devices  10.4 us (3%)
    all_gather x2, waiting for transfers between devices, side_by_side(): lax.all_gather(both, axis, axis=dim, tiled=True)  136 us
    all_to_all x2, waiting for transfers between devices, sum_at_owner(): tiles = lax.all_to_all(in_blocks(x, dim, length), axis, 0, 0, tiled=True)  61.2 us
    reduce_scatter x4, waiting for transfers between devices, sum_by_axis(): subtotal = lax.psum_scatter(subtotal, axis, scatter_dimension=0, tiled=True)  27.8 us
    all_gather x1, waiting for transfers between devices, body(): group = lax.all_gather(later_rows, 'tp', axis=0, tiled=True)  27.6 us
    dot_general x2, matrix products, contract_last(): lax.dot_general(left, right, (((1,), (1,)), ((), ())), preferred_element_...  15.9 us
    all_to_all x2, starting transfers between devices, sum_at_owner(): tiles = lax.all_to_all(in_blocks(x, dim, length), axis, 0, 0, tiled=True)  10.1 us
    dot_general x2, matrix products, grad_owner(): lax.dot_general(group, right, (((0,), (0,)), ((), ())), preferred_element...  9.68 us
    reduce_sum x2, other arithmetic, sum_at_owner(): return jnp.sum(tiles.astype(jnp.float32), axis=0)  7.73 us
  transfers between devices with their start and end apart: 9, of which 7 were waited for; matrix products, arithmetic and copies ran while one was open for 14% of the time, Pallas kernels for 0%

commit v1 on v0

v1 whole, which is shorter than its diff:
```python
import math
from types import SimpleNamespace

import jax
import jax.numpy as jnp
from jax import lax
from jax.experimental import pallas as pl
from jax.experimental.pallas import tpu as pltpu
from jax.sharding import PartitionSpec as P

NZ, NX, NY = 8, 4, 4
BF = jnp.bfloat16
F32 = jnp.float32
N_COPIES = 160


def scratch_of(tok, d, ff, rows):
    per_z = NX * rows
    vm = pltpu.VMEM
    return dict(
        ye=vm((4 * tok, d), BF),
        yc=vm((4 * tok, d), BF),
        yl=vm((4 * tok, d), BF),
        wu=vm((2, NZ, per_z, ff), BF),
        wd=vm((2, NZ, per_z, ff), BF),
        hid=vm((4 * tok, 2 * ff), BF),
        pg=vm((4 * tok, 2 * ff), BF),
        pe=vm((4 * tok, d), BF),
        po=vm((4 * tok, d), BF),
        se=vm((2, tok // 2, d), BF),
        so=vm((2, tok // 2, d), BF),
        re=vm((2, tok, d), BF),
        ro=vm((2, tok, d), BF),
        gou=vm((NZ, per_z, ff), BF),
        god=vm((NZ, per_z, ff), BF),
        xu=vm((NZ, per_z, ff), BF),
        xd=vm((NZ, per_z, ff), BF),
        su=vm((NZ, per_z, ff), BF),
        sd=vm((NZ, per_z, ff), BF),
        sx=vm((2, NZ // 2, rows, ff), BF),
        rx=vm((2, NZ, rows, ff), BF),
        tu=vm((NZ, rows, ff), BF),
        rz=vm((NZ - 1, rows, ff), BF),
        ra=vm((4, per_z, ff), BF),
        rb=vm((4, per_z, ff), BF),
        td=vm((NX, rows, ff), BF),
        rxd=vm((NX - 1, rows, ff), BF),
        tot_u=vm((rows, ff), F32),
        tot_d=vm((rows, ff), F32),
        send=pltpu.SemaphoreType.DMA((N_COPIES,)),
        recv=pltpu.SemaphoreType.DMA((N_COPIES,)),
        local=pltpu.SemaphoreType.DMA((16,)),
    )


def dot_tt(a, b):
    return lax.dot_general(a, b, (((1,), (1,)), ((), ())), preferred_element_type=F32)


def dot_ta(a, b):
    return lax.dot_general(a, b, (((0,), (0,)), ((), ())), preferred_element_type=F32)


def kernel(names, factor, *refs):
    later, earlier, cot, up, down, up_total, down_total = refs[:7]
    o_later, o_earlier, o_up, o_down = refs[7:11]
    r = SimpleNamespace(**dict(zip(names, refs[11:])))
    tok, d = later.shape
    rows, ff = up.shape
    half = tok // 2
    per_z = NX * rows
    hz = per_z // 2

    f, t = lax.axis_index("fs"), lax.axis_index("tp")
    z, x = f // NX, f % NX
    y, c = t // 2, t % 2

    def zi(k):
        return (z + k + NZ) % NZ

    def xi(k):
        return (x + k + NX) % NX

    def dev(dz=0, dx=0, dy=0, dc=0):
        fs = zi(dz) * NX + xi(dx)
        tp = ((y + dy + NY) % NY) * 2 + (c + dc) % 2
        return {"fs": fs, "tp": tp}

    sent = []

    def send(src, dst, to):
        i = len(sent)
        copy = pltpu.make_async_remote_copy(
            src_ref=src,
            dst_ref=dst,
            send_sem=r.send.at[i],
            recv_sem=r.recv.at[i],
            device_id=to,
            device_id_type=pl.DeviceIdType.MESH,
        )
        copy.start()
        sent.append(copy)
        return copy

    def got(*copies):
        for copy in copies:
            copy.wait_recv()

    local = []

    def fetch(src, dst):
        copy = pltpu.make_async_copy(src, dst, r.local.at[len(local)])
        copy.start()
        local.append(copy)
        return copy

    def xs(k):
        return pl.ds(pl.multiple_of(xi(k) * rows, rows), rows)

    first = [
        fetch(earlier, r.ye.at[pl.ds(0, tok)]),
        fetch(cot, r.yc.at[pl.ds(0, tok)]),
        fetch(up, r.wu.at[0, z, xs(0)]),
        fetch(down, r.wd.at[0, z, xs(0)]),
        fetch(later, r.yl.at[pl.ds(0, tok)]),
    ]
    totals = [fetch(up_total, r.tot_u), fetch(down_total, r.tot_d)]

    barrier = pltpu.get_barrier_semaphore()
    partners = [dev(dy=1), dev(dy=-1), dev(dc=1), dev(dx=1), dev(dx=2), dev(dx=3)]
    partners += [dev(dz=k) for k in range(1, NZ)]
    for p in partners:
        pl.semaphore_signal(barrier, inc=1, device_id=p, device_id_type=pl.DeviceIdType.MESH)
    pl.semaphore_wait(barrier, len(partners))
    for copy in first:
        copy.wait()

    def rows_of(slot, h):
        return pl.ds(slot * tok + h * half, half)

    def own_tokens(buf, h):
        plus = send(buf.at[rows_of(0, h)], buf.at[rows_of(1, h)], dev(dy=1))
        minus = send(buf.at[rows_of(0, 1 - h)], buf.at[rows_of(2, 1 - h)], dev(dy=-1))
        return plus, minus

    def pass_tokens(buf, pair):
        got(*pair)
        plus = send(buf.at[rows_of(1, 0)], buf.at[rows_of(3, 0)], dev(dy=1))
        minus = send(buf.at[rows_of(2, 1)], buf.at[rows_of(3, 1)], dev(dy=-1))
        return plus, minus

    wu, wd = r.wu, r.wd

    def up_block(dz, dx):
        return wu.at[0, zi(dz), xs(dx)]

    def up_z(dz, step, h=None):
        ref = up_block(dz, 0)
        if h is not None:
            ref = ref.at[pl.ds(h * (rows // 2), rows // 2)]
        return send(ref, ref, dev(dz=step))

    up_x = {}

    def up_to_x(dz):
        ref = up_block(dz, 0)
        up_x[dz] = (send(ref, ref, dev(dx=1)), send(ref, ref, dev(dx=-1)))

    def up_pass_x(dz):
        plus, minus = up_x[dz]
        if 0 <= dz <= 3:
            got(plus)
            ref = up_block(dz, -1)
            return send(ref, ref, dev(dx=1)), minus
        got(minus)
        ref = up_block(dz, 1)
        return send(ref, ref, dev(dx=-1)), plus

    def up_column(dx):
        src = wu.at[0, :, xs(dx)]
        return send(src, wu.at[1, :, xs(dx)], dev(dc=1))

    def down_half(dz, h):
        return wd.at[0, zi(dz), pl.ds(h * hz, hz)]

    def down_z(dz, step, h):
        ref = down_half(dz, h)
        return send(ref, ref, dev(dz=step))

    def down_chunk(dz):
        return send(wd.at[0, zi(dz)], wd.at[1, zi(dz)], dev(dc=1))

    e_a = own_tokens(r.ye, 0)
    c_a = own_tokens(r.yc, 0)
    e_b = own_tokens(r.ye, 1)
    c_b = own_tokens(r.yc, 1)
    own_down = wd.at[0, z, xs(0)]
    down_x = [send(own_down, own_down, dev(dx=k)) for k in (1, -1, 2)]
    zp, zm = [up_z(0, 1)], [up_z(0, -1)]
    up_to_x(0)

    across = []
    got(zp[0], zm[0])
    zp.append(up_z(-1, 1))
    zm.append(up_z(1, -1))
    got(*down_x)
    dp = [(down_z(0, 1, 0), down_z(0, 1, 1))]
    dm = [(down_z(0, -1, 1), down_z(0, -1, 0))]
    across.append(down_chunk(0))
    up_to_x(-1)
    up_to_x(1)
    got(zp[1], zm[1])
    zp.append(up_z(-2, 1))
    zm.append(up_z(2, -1))
    up_to_x(-2)
    up_to_x(2)
    last_up = [up_pass_x(0)]

    def down_pass(k):
        dp_new, dm_new = [], []
        for i in range(2):
            got(dp[k - 1][i])
            if k < 3 or i == 0:
                dp_new.append(down_z(-k, 1, i))
            got(dm[k - 1][i])
            if k < 3 or i == 0:
                dm_new.append(down_z(k, -1, 1 - i))
        dp.append(dp_new)
        dm.append(dm_new)
        across.append(down_chunk(-k))
        across.append(down_chunk(k))

    got(zp[2], zm[2])
    zp.append(up_z(-3, 1, 0))
    zm.append(up_z(3, -1, 1))
    up_to_x(-3)
    up_to_x(3)
    down_pass(1)
    last_up += [up_pass_x(-1), up_pass_x(1)]
    e_f = pass_tokens(r.ye, e_a)
    c_f = pass_tokens(r.yc, c_a)
    l_a = own_tokens(r.yl, 0)
    l_b = own_tokens(r.yl, 1)
    got(zp[3], zm[3])
    up_to_x(4)
    across.append(up_column(0))
    last_up += [up_pass_x(-2), up_pass_x(2)]
    down_pass(2)
    last_up += [up_pass_x(-3), up_pass_x(3)]
    last_up += [up_pass_x(4)]
    for passed, other in last_up:
        got(other)
    across.append(up_column(-1))
    across.append(up_column(1))
    down_pass(3)
    for passed, other in last_up:
        got(passed)
    across.append(up_column(2))
    got(dp[3][0], dm[3][0])
    across.append(down_chunk(4))
    got(*across)
    got(*e_b, *c_b, *e_f, *c_f)

    tile = 256
    for core in range(2):

        @pl.loop(0, ff // tile)
        def _(n):
            at = pl.multiple_of(n * tile, tile)
            w_up = wu[core, :, :, pl.ds(at, tile)].reshape(d, tile)
            w_down = wd[core, :, :, pl.ds(at, tile)].reshape(d, tile)
            relu = jnp.maximum(jnp.dot(r.ye[...], w_up, preferred_element_type=F32), 0.0)
            grad = jnp.dot(r.yc[...], w_down, preferred_element_type=F32)
            out = pl.ds(pl.multiple_of(core * ff + at, tile), tile)
            r.hid[:, out] = (relu * relu).astype(BF)
            r.pg[:, out] = (2.0 * relu * grad).astype(BF)

    def cross_grad(left, right, out, into):
        copies = []
        for part in range(2):

            @pl.loop(part * NZ // 2, (part + 1) * NZ // 2)
            def _(k):
                cols = pl.ds(pl.multiple_of(k * per_z, per_z), per_z)
                out[k] = dot_ta(left[:, cols], right[:, ff:]).astype(BF)

            piece = pl.ds(part * NZ // 2, NZ // 2)
            copies.append(send(out.at[piece], into.at[piece], dev(dc=1)))
        return copies

    def own_grad(left, right, other, out):
        @pl.loop(0, NZ)
        def _(k):
            cols = pl.ds(pl.multiple_of(k * per_z, per_z), per_z)
            mine = dot_ta(left[:, cols], right[:, :ff])
            out[k] = (mine + other[k].astype(F32)).astype(BF)

    c_up = cross_grad(r.ye, r.pg, r.gou, r.xu)
    c_down = cross_grad(r.yc, r.hid, r.god, r.xd)
    l_f = pass_tokens(r.yl, l_a)
    got(*c_up)
    own_grad(r.ye, r.pg, r.xu, r.su)

    su, sd = r.su, r.sd
    nh = NZ // 2
    lo, hi = pl.ds(0, nh), pl.ds(nh, nh)
    ux_a = send(su.at[lo, xs(2)], r.sx.at[0], dev(dx=1))
    ux_b = send(su.at[hi, xs(2)], r.sx.at[1], dev(dx=-1))
    ur_a = [send(su.at[hi, xs(1)], r.rx.at[0, hi], dev(dx=1))]
    ur_b = [send(su.at[lo, xs(-1)], r.rx.at[1, lo], dev(dx=-1))]

    got(*c_down)
    own_grad(r.yc, r.hid, r.xd, r.sd)

    h0, h1 = pl.ds(0, hz), pl.ds(hz, hz)
    da = {(0, 0): send(sd.at[zi(4), h0], r.ra.at[0, h0], dev(dz=1))}
    db = {(0, 1): send(sd.at[zi(-4), h1], r.rb.at[0, h1], dev(dz=-1))}
    da[1, 1] = send(sd.at[zi(3), h1], r.ra.at[1, h1], dev(dz=1))
    db[1, 0] = send(sd.at[zi(-3), h0], r.rb.at[1, h0], dev(dz=-1))

    def hop(s, h, plus):
        part = pl.ds(h * hz, hz)
        arrived, buf, to = (da, r.ra, 1) if plus else (db, r.rb, -1)
        k = zi(4 - s) if plus else zi(s - 4)
        got(arrived[s - 1, h])
        total = sd[k, part].astype(F32) + buf[s - 1, part].astype(F32)
        sd[k, part] = total.astype(BF)
        arrived[s, h] = send(sd.at[k, part], buf.at[s, part], dev(dz=to))

    def back(left, weight, out):
        @pl.loop(0, NZ)
        def _(k):
            acc = dot_tt(left[:, :ff], weight[0, k]) + dot_tt(left[:, ff:], weight[1, k])
            out[:, pl.ds(pl.multiple_of(k * per_z, per_z), per_z)] = acc.astype(BF)

    def start_sum(p, s, m):
        a = send(p.at[rows_of(3, 0)], s.at[0], dev(dy=1))
        b = send(p.at[rows_of(3, 1)], s.at[1], dev(dy=-1))
        ra = send(p.at[rows_of(2, 1)], m.at[0, pl.ds(half, half)], dev(dy=1))
        rb = send(p.at[rows_of(1, 0)], m.at[1, pl.ds(0, half)], dev(dy=-1))
        return a, b, ra, rb

    def pass_sum(p, s, m, pieces):
        a, b, ra, rb = pieces
        got(a)
        at = rows_of(2, 0)
        p[at] = (p[at].astype(F32) + s[0].astype(F32)).astype(BF)
        ra2 = send(p.at[at], m.at[0, pl.ds(0, half)], dev(dy=1))
        got(b)
        at = rows_of(1, 1)
        p[at] = (p[at].astype(F32) + s[1].astype(F32)).astype(BF)
        rb2 = send(p.at[at], m.at[1, pl.ds(half, half)], dev(dy=-1))
        return ra, rb, ra2, rb2

    def end_sum(p, m, pieces, out):
        got(*pieces)
        own = pl.ds(0, tok)
        total = p[own].astype(F32) + m[0].astype(F32) + m[1].astype(F32)
        p[own] = total.astype(BF)
        return fetch(p.at[own], out)

    back(r.pg, wu, r.pe)
    y_e = start_sum(r.pe, r.se, r.re)

    got(ux_a)
    su[lo, xs(1)] = (su[lo, xs(1)].astype(F32) + r.sx[0].astype(F32)).astype(BF)
    ur_a.append(send(su.at[lo, xs(1)], r.rx.at[0, lo], dev(dx=1)))
    got(ux_b)
    su[hi, xs(-1)] = (su[hi, xs(-1)].astype(F32) + r.sx[1].astype(F32)).astype(BF)
    ur_b.append(send(su.at[hi, xs(-1)], r.rx.at[1, hi], dev(dx=-1)))
    hop(1, 0, True)
    hop(1, 1, False)

    got(*l_b, *l_f)
    for core in range(2):

        @pl.loop(0, ff // tile)
        def _(n):
            at = pl.multiple_of(n * tile, tile)
            w_up = wu[core, :, :, pl.ds(at, tile)].reshape(d, tile)
            relu = jnp.maximum(jnp.dot(r.yl[...], w_up, preferred_element_type=F32), 0.0)
            out = pl.ds(pl.multiple_of(core * ff + at, tile), tile)
            r.hid[:, out] = (relu * relu).astype(BF)

    hop(2, 1, True)
    hop(2, 0, False)
    y_e = pass_sum(r.pe, r.se, r.re, y_e)
    back(r.hid, wd, r.po)
    y_o = start_sum(r.po, r.so, r.ro)

    hop(2, 0, True)
    hop(2, 1, False)
    hop(3, 1, True)
    hop(3, 0, False)
    got(*ur_a, *ur_b)
    tu = r.tu
    tu[...] = (
        su[:, xs(0)].astype(F32) + r.rx[0].astype(F32) + r.rx[1].astype(F32)
    ).astype(BF)
    uz = [send(tu.at[zi(k)], r.rz.at[k - 1], dev(dz=k)) for k in (1, 7, 2, 6, 3, 5, 4)]
    hop(3, 0, True)
    hop(3, 1, False)

    out_e = end_sum(r.pe, r.re, y_e, o_earlier)
    y_o = pass_sum(r.po, r.so, r.ro, y_o)

    got(da[3, 0], da[3, 1], db[3, 0], db[3, 1])
    down_sum = sd[z].astype(F32) + r.ra[3].astype(F32) + r.rb[3].astype(F32)
    r.td[...] = down_sum.astype(BF).reshape(NX, rows, ff)
    dx = [send(r.td.at[xi(k)], r.rxd.at[k - 1], dev(dx=k)) for k in (1, 3, 2)]

    for copy in totals:
        copy.wait()
    got(*uz)
    total = tu[z].astype(F32)
    for k in range(NZ - 1):
        total = total + r.rz[k].astype(F32)
    r.tot_u[...] = r.tot_u[...] + total * factor
    out_u = fetch(r.tot_u, o_up)
    got(*dx)
    total = r.td[x].astype(F32)
    for k in range(NX - 1):
        total = total + r.rxd[k].astype(F32)
    r.tot_d[...] = r.tot_d[...] + total * factor
    out_d = fetch(r.tot_d, o_down)

    out_l = end_sum(r.po, r.ro, y_o, o_later)
    for copy in sent:
        copy.wait_send()
    for copy in (out_e, out_u, out_d, out_l):
        copy.wait()


def body(later_rows, earlier_rows, cotangent, up_weight, down_weight, up_total, down_total):
    tok, d = later_rows.shape
    rows, ff = up_weight.shape
    total_rows = tok * lax.axis_size("fs") * lax.axis_size("tp")
    factor = 1.0 / math.sqrt(total_rows)
    scratch = scratch_of(tok, d, ff, rows)

    def run(*refs):
        kernel(list(scratch), factor, *refs)

    return pl.pallas_call(
        run,
        out_shape=(
            jax.ShapeDtypeStruct((tok, d), BF),
            jax.ShapeDtypeStruct((tok, d), BF),
            jax.ShapeDtypeStruct((rows, ff), F32),
            jax.ShapeDtypeStruct((rows, ff), F32),
        ),
        in_specs=[pl.BlockSpec(memory_space=pl.ANY)] * 7,
        out_specs=(pl.BlockSpec(memory_space=pl.ANY),) * 4,
        scratch_shapes=list(scratch.values()),
        compiler_params=pltpu.CompilerParams(
            collective_id=0, has_side_effects=True, vmem_limit_bytes=67_000_000
        ),
        name="ffn_step",
    )(later_rows, earlier_rows, cotangent, up_weight, down_weight, up_total, down_total)


def solution(mesh):
    tokens = P(("fs", "tp"), None)
    weight = P("fs", "tp")
    return jax.shard_map(
        body,
        mesh=mesh,
        in_specs=(tokens, tokens, tokens, weight, weight, weight, weight),
        out_specs=(tokens, tokens, weight, weight),
        check_vma=False,
    )
```

time: 331 us -> 114 us (0.34)
  waiting for transfers between devices: 254 us -> 0 us
  Pallas kernels: 0 us -> 107 us
  matrix products: 36.1 us -> 0 us
  other arithmetic: 14.6 us -> 0 us
  between operations: 14.2 us -> 0.65 us
  starting transfers between devices: 10.4 us -> 0 us
  local copies, waits for them, and re-layouts: 0.02 us -> 4.57 us
    all_gather x3 -> x0, waiting for transfers between devices: 164 us -> none  [the longest x2 136 us: side_by_side(): lax.all_gather(both, axis, axis=dim, tiled=True)]
    pallas_call x0 -> x1, Pallas kernels: none -> 107 us  [body(): pl.pallas_call(run, out_shape=(jax.ShapeDtypeStruct((tok, d), BF), jax.Sh...]
    all_to_all x2 -> x0, waiting for transfers between devices: 61.2 us -> none  [sum_at_owner(): tiles = lax.all_to_all(in_blocks(x, dim, length), axis, 0, 0, tiled=True)]
    dot_general x6 -> x0, matrix products: 36.1 us -> none  [the longest x2 15.9 us: contract_last(): lax.dot_general(left, right, (((1,), (1,)), ((), ())), preferred_element_...]
    reduce_scatter x4 -> x0, waiting for transfers between devices: 27.8 us -> none  [sum_by_axis(): subtotal = lax.psum_scatter(subtotal, axis, scatter_dimension=0, tiled=True)]
    all_to_all x2 -> x0, starting transfers between devices: 10.1 us -> none  [sum_at_owner(): tiles = lax.all_to_all(in_blocks(x, dim, length), axis, 0, 0, tiled=True)]
    reduce_sum x2 -> x0, other arithmetic: 7.73 us -> none  [sum_at_owner(): return jnp.sum(tiles.astype(jnp.float32), axis=0)]
    unnamed x6 -> x10, local copies, waits for them, and re-layouts: 0.02 us -> 4.57 us
  transfers between devices with their start and end apart: 9 -> 0, of which waited for: 7 -> 0; matrix products, arithmetic and copies ran while one was open for 14% -> 0% of each run, Pallas kernels for 0% -> 0%
where the time goes in v1:
time: 114 us; the launch traced here: 113 us
  Pallas kernels  107 us (94%)
  local copies, waits for them, and re-layouts  4.57 us (4%)
    pallas_call x1, Pallas kernels, body(): pl.pallas_call(run, out_shape=(jax.ShapeDtypeStruct((tok, d), BF), jax.Sh...  107 us
    unnamed x10, local copies, waits for them, and re-layouts  4.57 us

profile of v1, /device:TPU:1, one launch (start us, length us, event | category | flops | bytes accessed | tf_op | source)
XLA Modules:
  0.0 112.7 jit_solution(13450656841883192041)
XLA Ops:
  0.6 107.4 %ffn_step.1 = (bf16[128,2048]{1,0:T(8,128)(2,1)}, bf16[128,2048]{1,0:T(8,128)(2,1)}, f32[64,512]{1,0:T(8,128)}, f32[64,512]{1,0:T(8,128)}) custom-call(bf16[128,2048]{1,0:T(8,128)(2,1)} %refs_0_.1, bf16[128,2048]{1,0:T(8,128)(2,1)} %refs_1_.1, bf16[128,2048]{1,0:T(8,128)(2,1)} %refs_2_.1, bf16[64,512]{1,0:T(8,128)(2,1)} %refs_3_.1, bf16[64,512]{1,0:T(8,128)(2,1)} %refs_4_.1, ...), custom_call_target="tpu_custom_call" | custom-call | tf_op jit(solution)/shard_map/ffn_step/pallas_call | solution.py:444
  108.1 0.0 copy-start
  108.1 1.9 %copy.15 = bf16[128,2048]{1,0:T(8,128)(2,1)} copy(bf16[128,2048]{1,0:T(8,128)(2,1)} %get-tuple-element.8) | data formatting | bytes 1048576
  110.0 0.0 copy-done
  110.0 0.0 copy-start.2
  110.0 0.8 copy.16
  110.8 0.2 copy-done.2
  111.1 0.0 copy-start.1
  111.1 0.7 copy.17
  111.7 0.3 copy-done.1
  112.0 0.7 copy.18
Async XLA Ops:
  108.1 2.0 %copy-start = (bf16[128,2048]{1,0:T(8,128)(2,1)S(1)}, bf16[128,2048]{1,0:T(8,128)(2,1)}, u32[]{:S(2)}) copy-start(bf16[128,2048]{1,0:T(8,128)(2,1)} %get-tuple-element.9) | copy-start | bytes 1572868
  110.0 1.0 copy-start.2
  111.1 1.0 copy-start.1

commit v2 on v0

v2 whole, which is shorter than its diff:
```python
import math
from types import SimpleNamespace

import jax
import jax.numpy as jnp
from jax import lax
from jax.experimental import pallas as pl
from jax.experimental.pallas import tpu as pltpu
from jax.sharding import PartitionSpec as P

NZ, NX, NY = 8, 4, 4
BF = jnp.bfloat16
F32 = jnp.float32
N_SENT = 13
N_GOT = 68


def scratch_of(tok, d, ff, rows):
    per_z = NX * rows
    vm = pltpu.VMEM
    return dict(
        ye=vm((4 * tok, d), BF),
        yc=vm((4 * tok, d), BF),
        yl=vm((4 * tok, d), BF),
        wu=vm((2, NZ, per_z, ff), BF),
        wd=vm((2, NZ, per_z, ff), BF),
        hid=vm((4 * tok, 2 * ff), BF),
        rel=vm((tok, 2 * ff), F32),
        pg=vm((4 * tok, 2 * ff), BF),
        pe=vm((4 * tok, d), BF),
        po=vm((4 * tok, d), BF),
        se=vm((2, tok // 2, d), BF),
        so=vm((2, tok // 2, d), BF),
        re=vm((2, tok, d), BF),
        ro=vm((2, tok, d), BF),
        gou=vm((NZ, per_z, ff), BF),
        god=vm((NZ, per_z, ff), BF),
        xu=vm((NZ, per_z, ff), BF),
        xd=vm((NZ, per_z, ff), BF),
        su=vm((NZ, per_z, ff), BF),
        sd=vm((NZ, per_z, ff), BF),
        sx=vm((2, NZ // 2, rows, ff), BF),
        rx=vm((2, NZ, rows, ff), BF),
        tu=vm((NZ, rows, ff), BF),
        ua=vm((4, rows, ff), BF),
        ub=vm((4, rows, ff), BF),
        ra=vm((4, per_z, ff), BF),
        rb=vm((4, per_z, ff), BF),
        td=vm((NX, rows, ff), BF),
        xa=vm((2, rows, ff), BF),
        xb=vm((2, rows, ff), BF),
        et=vm((d, 4 * tok), BF),
        ct=vm((d, 4 * tok), BF),
        tot_u=vm((rows, ff), F32),
        tot_d=vm((rows, ff), F32),
        send=pltpu.SemaphoreType.DMA((N_SENT,)),
        recv=pltpu.SemaphoreType.DMA((N_GOT,)),
        local=pltpu.SemaphoreType.DMA((7,)),
    )


def dot_tt(a, b):
    return lax.dot_general(a, b, (((1,), (1,)), ((), ())), preferred_element_type=F32)


def kernel(names, factor, *refs):
    later, earlier, cot, up, down, up_total, down_total = refs[:7]
    o_later, o_earlier, o_up, o_down = refs[7:11]
    r = SimpleNamespace(**dict(zip(names, refs[11:])))
    tok, d = later.shape
    rows, ff = up.shape
    half = tok // 2
    per_z = NX * rows
    hz = per_z // 2

    f, t = lax.axis_index("fs"), lax.axis_index("tp")
    z, x = f // NX, f % NX
    y, c = t // 2, t % 2

    def zi(k):
        return (z + k + NZ) % NZ

    def xi(k):
        return (x + k + NX) % NX

    def dev(dz=0, dx=0, dy=0, dc=0):
        fs = zi(dz) * NX + xi(dx)
        tp = ((y + dy + NY) % NY) * 2 + (c + dc) % 2
        return {"fs": fs, "tp": tp}

    row_bytes = d * 2
    limit = r.ye.shape[0] * row_bytes
    leaving, arriving = [], []

    def group():
        g = SimpleNamespace(at=len(arriving), bytes=0)
        arriving.append(g)
        return g

    def wait(sem, g):
        ref = r.ye.at[pl.ds(0, g.bytes // row_bytes)]
        pltpu.make_async_copy(ref, ref, sem).wait()

    def send(src, dst, to, g=None):
        size = math.prod(src.shape) * 2
        g = group() if g is None else g
        g.bytes += size
        if not leaving or leaving[-1].done or leaving[-1].bytes + size > limit:
            leaving.append(SimpleNamespace(bytes=0, done=False))
        leaving[-1].bytes += size
        pltpu.make_async_remote_copy(
            src_ref=src,
            dst_ref=dst,
            send_sem=r.send.at[len(leaving) - 1],
            recv_sem=r.recv.at[g.at],
            device_id=to,
            device_id_type=pl.DeviceIdType.MESH,
        ).start()
        return g

    @jax.named_scope("sent")
    def settle():
        for i, g in enumerate(leaving):
            if not g.done:
                wait(r.send.at[i], g)
                g.done = True

    def got(name, *groups):
        with jax.named_scope(name):
            for g in {g.at: g for g in groups}.values():
                wait(r.recv.at[g.at], g)

    local = []

    def fetch(src, dst):
        copy = pltpu.make_async_copy(src, dst, r.local.at[len(local)])
        copy.start()
        local.append(copy)
        return copy

    def xs(k):
        return pl.ds(pl.multiple_of(xi(k) * rows, rows), rows)

    first = [
        fetch(earlier, r.ye.at[pl.ds(0, tok)]),
        fetch(cot, r.yc.at[pl.ds(0, tok)]),
        fetch(up, r.wu.at[0, z, xs(0)]),
        fetch(down, r.wd.at[0, z, xs(0)]),
        fetch(later, r.yl.at[pl.ds(0, tok)]),
    ]
    totals = [fetch(up_total, r.tot_u), fetch(down_total, r.tot_d)]

    barrier = pltpu.get_barrier_semaphore()
    partners = [dev(dy=1), dev(dy=-1), dev(dx=1), dev(dx=-1), dev(dz=1), dev(dz=-1), dev(dc=1)]
    for p in partners:
        pl.semaphore_signal(barrier, inc=1, device_id=p, device_id_type=pl.DeviceIdType.MESH)
    with jax.named_scope("barrier"):
        pl.semaphore_wait(barrier, len(partners))
        for copy in first:
            copy.wait()

    def rows_of(slot, h):
        return pl.ds(slot * tok + h * half, half)

    def own_tokens(buf, h, g=None):
        g = g or group()
        send(buf.at[rows_of(0, h)], buf.at[rows_of(1, h)], dev(dy=1), g)
        send(buf.at[rows_of(0, 1 - h)], buf.at[rows_of(2, 1 - h)], dev(dy=-1), g)
        return g

    def pass_tokens(buf, first, g=None):
        g = g or group()
        got("tok_first", first)
        send(buf.at[rows_of(1, 0)], buf.at[rows_of(3, 0)], dev(dy=1), g)
        send(buf.at[rows_of(2, 1)], buf.at[rows_of(3, 1)], dev(dy=-1), g)
        return g

    wu, wd = r.wu, r.wd

    def up_block(dz, dx):
        return wu.at[0, zi(dz), xs(dx)]

    def up_z(k):
        g = group()
        for step in (1, -1):
            ref = up_block(-k * step, 0)
            if k == 3:
                ref = ref.at[pl.ds(0 if step == 1 else rows // 2, rows // 2)]
            send(ref, ref, dev(dz=step), g)
        return g

    up_first, up_rest, up_last = {}, group(), group()

    def up_to_x(dz):
        ref = up_block(dz, 0)
        up_first[dz] = group()
        plus, minus = (up_first[dz], up_rest) if 0 <= dz <= 3 else (up_rest, up_first[dz])
        send(ref, ref, dev(dx=1), plus)
        send(ref, ref, dev(dx=-1), minus)

    def up_pass_x(*dzs):
        for dz in dzs:
            got("up_x", up_first[dz])
            step = 1 if 0 <= dz <= 3 else -1
            ref = up_block(dz, -step)
            send(ref, ref, dev(dx=step), up_last)

    across_up, across_down = group(), group()

    def up_column(dx):
        src = wu.at[0, :, xs(dx)]
        send(src, wu.at[1, :, xs(dx)], dev(dc=1), across_up)

    def down_block(dz, dx):
        return wd.at[0, zi(dz), xs(dx)]

    down_far = group()
    down_at = {}

    def down_z(k, *dxs):
        for dx in dxs:
            g = down_far if k == 3 else group()
            down_at[k + 1, dx] = g
            if k < 3 or dx in (0, -1):
                ref = down_block(-k, dx)
                send(ref, ref, dev(dz=1), g)
            if k < 3 or dx in (1, 2):
                ref = down_block(k, dx)
                send(ref, ref, dev(dz=-1), g)

    def down_pass(k, *dxs):
        for dx in dxs:
            got(f"down_z{k}", down_at[k, dx])
            down_z(k, dx)

    def down_chunk(*dzs):
        for dz in dzs:
            send(wd.at[0, zi(dz)], wd.at[1, zi(dz)], dev(dc=1), across_down)

    @jax.named_scope("turn")
    def turn(slot, src, dst):
        @pl.loop(0, NZ)
        def _(k):
            cols = pl.ds(pl.multiple_of(k * per_z, per_z), per_z)
            dst[cols, pl.ds(slot * tok, tok)] = src[pl.ds(slot * tok, tok), cols].T

    e_a = own_tokens(r.ye, 0)
    up_1 = up_z(0)
    own_down = down_block(0, 0)
    down_x1, down_x2 = group(), group()
    send(own_down, own_down, dev(dx=1), down_x1)
    send(own_down, own_down, dev(dx=-1), down_x1)
    down_z(0, 0)
    up_to_x(0)
    c_a = own_tokens(r.yc, 0)
    tok_own = own_tokens(r.ye, 1)
    own_tokens(r.yc, 1, tok_own)
    turn(0, r.ye, r.et)

    got("up_z1", up_1)
    up_2 = up_z(1)
    got("down_x", down_x1)
    part = down_block(0, -1).at[pl.ds(0, rows // 2)]
    send(part, part, dev(dx=1), down_x2)
    part = down_block(0, 1).at[pl.ds(rows // 2, rows // 2)]
    send(part, part, dev(dx=-1), down_x2)
    down_z(0, -1, 1)
    up_to_x(-1)
    up_to_x(1)
    down_pass(1, 0)
    turn(0, r.yc, r.ct)
    got("up_z2", up_2)
    up_3 = up_z(2)
    up_to_x(-2)
    up_to_x(2)
    got("down_x2", down_x2)
    down_z(0, 2)
    down_chunk(0)
    up_pass_x(0)
    down_pass(1, -1, 1)
    got("up_z3", up_3)
    up_4 = up_z(3)
    up_to_x(-3)
    up_to_x(3)
    down_pass(2, 0)
    up_pass_x(-1, 1)
    down_pass(1, 2)
    down_chunk(-1, 1)
    e_f = pass_tokens(r.ye, e_a)
    down_pass(2, -1, 1)
    got("up_z4", up_4)
    up_to_x(4)
    up_column(0)
    c_f = pass_tokens(r.yc, c_a)
    l_a = own_tokens(r.yl, 0)
    tok_l = own_tokens(r.yl, 1)
    up_pass_x(-2, 2)
    down_pass(3, 0)
    down_pass(2, 2)
    down_chunk(-2, 2)
    down_pass(3, -1, 1)
    up_pass_x(-3, 3, 4)
    got("up_x_rest", up_rest)
    up_column(-1)
    up_column(1)
    down_pass(3, 2)
    down_chunk(-3, 3)
    got("up_x_last", up_last)
    up_column(2)
    got("down_z4", down_far)
    down_chunk(4)
    got("tok_own", tok_own)
    for slot in (1, 2):
        turn(slot, r.ye, r.et)
        turn(slot, r.yc, r.ct)
    got("across", across_up, across_down)

    tile = 256
    many, last = pl.ds(0, 3 * tok), pl.ds(3 * tok, tok)

    @jax.named_scope("pre_earlier")
    def pre_earlier():
        for core in range(2):

            @pl.loop(0, ff // tile)
            def _(n):
                at = pl.multiple_of(n * tile, tile)
                w_up = wu[core, :, :, pl.ds(at, tile)].reshape(d, tile)
                w_down = wd[core, :, :, pl.ds(at, tile)].reshape(d, tile)
                relu = jnp.maximum(jnp.dot(r.ye[many], w_up, preferred_element_type=F32), 0.0)
                grad = jnp.dot(r.yc[many], w_down, preferred_element_type=F32)
                out = pl.ds(pl.multiple_of(core * ff + at, tile), tile)
                r.hid[many, out] = (relu * relu).astype(BF)
                r.pg[many, out] = (2.0 * relu * grad).astype(BF)

    @jax.named_scope("pre_last_e")
    def pre_last_e():
        for core in range(2):

            @pl.loop(0, ff // tile)
            def _(n):
                at = pl.multiple_of(n * tile, tile)
                w_up = wu[core, :, :, pl.ds(at, tile)].reshape(d, tile)
                relu = jnp.maximum(jnp.dot(r.ye[last], w_up, preferred_element_type=F32), 0.0)
                out = pl.ds(pl.multiple_of(core * ff + at, tile), tile)
                r.hid[last, out] = (relu * relu).astype(BF)
                r.rel[:, out] = relu

    @jax.named_scope("pre_last_c")
    def pre_last_c():
        for core in range(2):

            @pl.loop(0, ff // tile)
            def _(n):
                at = pl.multiple_of(n * tile, tile)
                w_down = wd[core, :, :, pl.ds(at, tile)].reshape(d, tile)
                grad = jnp.dot(r.yc[last], w_down, preferred_element_type=F32)
                out = pl.ds(pl.multiple_of(core * ff + at, tile), tile)
                r.pg[last, out] = (2.0 * r.rel[:, out] * grad).astype(BF)

    @jax.named_scope("pre_later")
    def pre_later(core):
        @pl.loop(0, ff // tile)
        def _(n):
            at = pl.multiple_of(n * tile, tile)
            w_up = wu[core, :, :, pl.ds(at, tile)].reshape(d, tile)
            relu = jnp.maximum(jnp.dot(r.yl[...], w_up, preferred_element_type=F32), 0.0)
            out = pl.ds(pl.multiple_of(core * ff + at, tile), tile)
            r.hid[:, out] = (relu * relu).astype(BF)

    pre_earlier()
    got("tok_last_e", e_f)
    turn(3, r.ye, r.et)
    pre_last_e()
    got("tok_last_c", c_f)
    turn(3, r.yc, r.ct)
    pre_last_c()

    def gradient(left, right, ks, core):
        rows_at = [left[pl.ds(pl.multiple_of(k * per_z, per_z), per_z)] for k in ks]
        both = jnp.concatenate(rows_at, axis=0)
        cols = right[:, core * ff : (core + 1) * ff]
        both = jnp.dot(both, cols, preferred_element_type=F32)
        return both[:per_z], both[per_z:]

    def farthest(j):
        return zi(4 + (1 - 2 * (j % 2)) * ((j + 1) // 2))

    @jax.named_scope("cross_grad")
    def cross_grad(left, right, out, into, order):
        copies = []
        for part in range(4):
            ks = order(2 * part), order(2 * part + 1)
            for k, total in zip(ks, gradient(left, right, ks, 1)):
                out[k] = total.astype(BF)
            g = group()
            for k in ks:
                send(out.at[k], into.at[k], dev(dc=1), g)
            copies.append(g)
        return copies

    @jax.named_scope("own_grad")
    def own_grad(left, right, other, out, order, part):
        ks = order(2 * part), order(2 * part + 1)
        for k, total in zip(ks, gradient(left, right, ks, 0)):
            out[k] = (total + other[k].astype(F32)).astype(BF)

    su, sd = r.su, r.sd
    c_down = cross_grad(r.ct, r.hid, r.god, r.xd, farthest)

    arrived = {(s, first): group() for s in range(3) for first in (True, False)}
    z_last = group()
    for first in (True, False):
        arrived[3, first] = z_last

    def z_send(s, first):
        g = arrived[s, first]
        for k, buf, step in ((zi(4 - s), r.ra, 1), (zi(s - 4), r.rb, -1)):
            part = pl.ds(0 if first == (step == 1) else hz, hz)
            send(sd.at[k, part], buf.at[s, part], dev(dz=step), g)

    def hop(s, first):
        got(f"hop{s}", arrived[s - 1, first])
        for k, buf, step in ((zi(4 - s), r.ra, 1), (zi(s - 4), r.rb, -1)):
            part = pl.ds(0 if first == (step == 1) else hz, hz)
            total = sd[k, part].astype(F32) + buf[s - 1, part].astype(F32)
            sd[k, part] = total.astype(BF)
        z_send(s, first)

    c_up = cross_grad(r.et, r.pg, r.gou, r.xu, lambda j: j)
    for part in range(4):
        got("c_down", c_down[part])
        own_grad(r.ct, r.hid, r.xd, sd, farthest, part)
        if part == 0:
            z_send(0, True)
        if part == 1:
            z_send(1, False)
        if part == 2:
            pass_tokens(r.yl, l_a, tok_l)

    nh = NZ // 2
    lo, hi = pl.ds(0, nh), pl.ds(nh, nh)
    ux_a, ux_b, ur = group(), group(), group()
    for part in range(4):
        got("c_up", c_up[part])
        own_grad(r.et, r.pg, r.xu, su, lambda j: j, part)
        if part == 1:
            send(su.at[lo, xs(2)], r.sx.at[0], dev(dx=1), ux_a)
    send(su.at[hi, xs(2)], r.sx.at[1], dev(dx=-1), ux_b)
    send(su.at[hi, xs(1)], r.rx.at[0, hi], dev(dx=1), ur)
    send(su.at[lo, xs(-1)], r.rx.at[1, lo], dev(dx=-1), ur)

    @jax.named_scope("back")
    def back(left, weight, out):
        @pl.loop(0, NZ // 2)
        def _(k):
            for core in range(2):
                w = weight[core, pl.ds(2 * k, 2)].reshape(2 * per_z, ff)
                acc = dot_tt(left[:, core * ff : (core + 1) * ff], w)
                total = acc if core == 0 else total + acc
            out[:, pl.ds(pl.multiple_of(k * 2 * per_z, per_z), 2 * per_z)] = total.astype(BF)

    def start_sum(p, s, m):
        g, g0, g1 = group(), group(), group()
        send(p.at[rows_of(3, 0)], s.at[0], dev(dy=1), g)
        send(p.at[rows_of(3, 1)], s.at[1], dev(dy=-1), g)
        send(p.at[rows_of(2, 1)], m.at[0, pl.ds(half, half)], dev(dy=1), g1)
        send(p.at[rows_of(1, 0)], m.at[1, pl.ds(0, half)], dev(dy=-1), g0)
        return g, g0, g1

    def pass_sum(p, s, m, groups):
        g, g0, g1 = groups
        got("sum_first", g)
        at = rows_of(2, 0)
        p[at] = (p[at].astype(F32) + s[0].astype(F32)).astype(BF)
        send(p.at[at], m.at[0, pl.ds(0, half)], dev(dy=1), g0)
        at = rows_of(1, 1)
        p[at] = (p[at].astype(F32) + s[1].astype(F32)).astype(BF)
        send(p.at[at], m.at[1, pl.ds(half, half)], dev(dy=-1), g1)

    def end_sum(p, m, groups, out):
        for h in range(2):
            got("sum_end", groups[1 + h])
            own = rows_of(0, h)
            total = p[own].astype(F32) + m[0, own].astype(F32) + m[1, own].astype(F32)
            out[own] = total.astype(BF)

    back(r.pg, wu, r.pe)
    y_e = start_sum(r.pe, r.se, r.re)
    hop(1, True)
    hop(2, False)

    got("tok_l", tok_l)
    pre_later(0)
    got("ux", ux_a)
    su[lo, xs(1)] = (su[lo, xs(1)].astype(F32) + r.sx[0].astype(F32)).astype(BF)
    send(su.at[lo, xs(1)], r.rx.at[0, lo], dev(dx=1), ur)
    hop(2, True)
    pre_later(1)
    got("ux", ux_b)
    su[hi, xs(-1)] = (su[hi, xs(-1)].astype(F32) + r.sx[1].astype(F32)).astype(BF)
    send(su.at[hi, xs(-1)], r.rx.at[1, hi], dev(dx=-1), ur)
    hop(3, False)
    back(r.hid, wd, r.po)
    pass_sum(r.pe, r.se, r.re, y_e)
    y_o = start_sum(r.po, r.so, r.ro)
    hop(3, True)

    got("hop4", z_last)
    down_sum = sd[z].astype(F32) + r.ra[3].astype(F32) + r.rb[3].astype(F32)
    td = r.td
    td[...] = down_sum.astype(BF).reshape(NX, rows, ff)
    q0, q1 = pl.ds(0, rows // 2), pl.ds(rows // 2, rows // 2)
    dx1, dx2 = group(), group()
    send(td.at[xi(2), q0], r.xa.at[0, q0], dev(dx=1), dx1)
    send(td.at[xi(2), q1], r.xb.at[0, q1], dev(dx=-1), dx1)

    got("ur", ur)
    tu = r.tu
    tu[...] = (
        su[:, xs(0)].astype(F32) + r.rx[0].astype(F32) + r.rx[1].astype(F32)
    ).astype(BF)
    uz = [group() for _ in range(4)]
    send(tu.at[zi(4), q0], r.ua.at[0, q0], dev(dz=1), uz[0])
    send(tu.at[zi(4), q1], r.ub.at[0, q1], dev(dz=-1), uz[0])

    def add_on(acc, k, buf, s, part):
        acc[k, part] = (acc[k, part].astype(F32) + buf[s, part].astype(F32)).astype(BF)

    def up_hop(s):
        got(f"uz{s}", uz[s - 1])
        whole = pl.ds(0, rows)
        add_on(tu, zi(4 - s), r.ua, s - 1, q0 if s == 1 else whole)
        send(tu.at[zi(4 - s)], r.ua.at[s], dev(dz=1), uz[s])
        add_on(tu, zi(s - 4), r.ub, s - 1, q1 if s == 1 else whole)
        send(tu.at[zi(s - 4)], r.ub.at[s], dev(dz=-1), uz[s])

    got("dx1", dx1)
    add_on(td, xi(1), r.xa, 0, q0)
    send(td.at[xi(1)], r.xa.at[1], dev(dx=1), dx2)
    add_on(td, xi(-1), r.xb, 0, q1)
    send(td.at[xi(-1)], r.xb.at[1], dev(dx=-1), dx2)
    up_hop(1)
    for copy in totals:
        copy.wait()
    got("dx2", dx2)
    total = td[x].astype(F32) + r.xa[1].astype(F32) + r.xb[1].astype(F32)
    o_down[...] = r.tot_d[...] + total * factor
    up_hop(2)
    pass_sum(r.po, r.so, r.ro, y_o)
    up_hop(3)
    end_sum(r.pe, r.re, y_e, o_earlier)
    got("uz4", uz[3])
    total = tu[z].astype(F32) + r.ua[3].astype(F32) + r.ub[3].astype(F32)
    o_up[...] = r.tot_u[...] + total * factor
    settle()
    end_sum(r.po, r.ro, y_o, o_later)
    assert len(leaving) == N_SENT and len(arriving) == N_GOT, (len(leaving), len(arriving))


def body(later_rows, earlier_rows, cotangent, up_weight, down_weight, up_total, down_total):
    given = later_rows, earlier_rows, cotangent, up_weight, down_weight, up_total, down_total
    tok, d = later_rows.shape
    rows, ff = up_weight.shape
    total_rows = tok * lax.axis_size("fs") * lax.axis_size("tp")
    factor = 1.0 / math.sqrt(total_rows)
    scratch = scratch_of(tok, d, ff, rows)

    def run(*refs):
        kernel(list(scratch), factor, *refs)

    shapes = (
        jax.ShapeDtypeStruct((tok, d), BF),
        jax.ShapeDtypeStruct((tok, d), BF),
        jax.ShapeDtypeStruct((rows, ff), F32),
        jax.ShapeDtypeStruct((rows, ff), F32),
    )
    results = pl.pallas_call(
        run,
        out_shape=shapes,
        in_specs=[pl.BlockSpec(memory_space=pltpu.HBM)] * 7,
        out_specs=(pl.BlockSpec(memory_space=pltpu.VMEM),) * 4,
        scratch_shapes=list(scratch.values()),
        compiler_params=pltpu.CompilerParams(
            collective_id=0, has_side_effects=True, vmem_limit_bytes=50 * 2**20
        ),
        name="ffn_step",
    )(*(pltpu.with_memory_space_constraint(a, pltpu.HBM) for a in given))
    return pl.pallas_call(
        store,
        out_shape=shapes,
        in_specs=[pl.BlockSpec(memory_space=pltpu.VMEM)] * 4,
        out_specs=(pl.BlockSpec(memory_space=pl.ANY),) * 4,
        scratch_shapes=[pltpu.SemaphoreType.DMA((4,))],
        compiler_params=pltpu.CompilerParams(vmem_limit_bytes=4 * 2**20),
        name="ffn_store",
    )(*results)


def store(*refs):
    copies = [pltpu.make_async_copy(refs[i], refs[4 + i], refs[8].at[i]) for i in range(4)]
    for copy in copies:
        copy.start()
    for copy in copies:
        copy.wait()


def solution(mesh):
    tokens = P(("fs", "tp"), None)
    weight = P("fs", "tp")
    return jax.shard_map(
        body,
        mesh=mesh,
        in_specs=(tokens, tokens, tokens, weight, weight, weight, weight),
        out_specs=(tokens, tokens, weight, weight),
        check_vma=False,
    )
```

time: 331 us -> 99.2 us (0.30)
  waiting for transfers between devices: 254 us -> 0 us
  Pallas kernels: 0 us -> 98.4 us
  matrix products: 36.1 us -> 0 us
  other arithmetic: 14.6 us -> 0 us
  between operations: 14.2 us -> 0.64 us
  starting transfers between devices: 10.4 us -> 0 us
    all_gather x3 -> x0, waiting for transfers between devices: 164 us -> none  [the longest x2 136 us: side_by_side(): lax.all_gather(both, axis, axis=dim, tiled=True)]
    pallas_call x0 -> x2, Pallas kernels: none -> 98.4 us  [the longest x1 97.4 us: body(): pl.pallas_call(run, out_shape=shapes, in_specs=[pl.BlockSpec(memory_space...]
    all_to_all x2 -> x0, waiting for transfers between devices: 61.2 us -> none  [sum_at_owner(): tiles = lax.all_to_all(in_blocks(x, dim, length), axis, 0, 0, tiled=True)]
    dot_general x6 -> x0, matrix products: 36.1 us -> none  [the longest x2 15.9 us: contract_last(): lax.dot_general(left, right, (((1,), (1,)), ((), ())), preferred_element_...]
    reduce_scatter x4 -> x0, waiting for transfers between devices: 27.8 us -> none  [sum_by_axis(): subtotal = lax.psum_scatter(subtotal, axis, scatter_dimension=0, tiled=True)]
    all_to_all x2 -> x0, starting transfers between devices: 10.1 us -> none  [sum_at_owner(): tiles = lax.all_to_all(in_blocks(x, dim, length), axis, 0, 0, tiled=True)]
    reduce_sum x2 -> x0, other arithmetic: 7.73 us -> none  [sum_at_owner(): return jnp.sum(tiles.astype(jnp.float32), axis=0)]
    concatenate x2 -> x0, other arithmetic: 3.82 us -> none  [side_by_side(): both = jnp.concatenate(arrays, axis=along)]
  transfers between devices with their start and end apart: 9 -> 0, of which waited for: 7 -> 0; matrix products, arithmetic and copies ran while one was open for 14% -> 0% of each run, Pallas kernels for 0% -> 0%
where the time goes in v2:
time: 99.2 us; the launch traced here: 99.1 us
  Pallas kernels  98.4 us (99%)
    pallas_call x1, Pallas kernels, body(): pl.pallas_call(run, out_shape=shapes, in_specs=[pl.BlockSpec(memory_space...  97.4 us

profile of v2, /device:TPU:1, one launch (start us, length us, event | category | flops | bytes accessed | tf_op | source)
XLA Modules:
  0.0 99.1 jit_solution(8313326036870599049)
XLA Ops:
  0.6 97.4 %ffn_step.1 = (bf16[128,2048]{1,0:T(8,128)(2,1)S(1)}, bf16[128,2048]{1,0:T(8,128)(2,1)S(1)}, f32[64,512]{1,0:T(8,128)S(1)}, f32[64,512]{1,0:T(8,128)S(1)}) custom-call(bf16[128,2048]{1,0:T(8,128)(2,1)} %refs_0_.1, bf16[128,2048]{1,0:T(8,128)(2,1)} %refs_1_.1, bf16[128,2048]{1,0:T(8,128)(2,1)} %refs_2_.1, bf16[64,512]{1,0:T(8,128)(2,1)} %refs_3_.1, ...), custom_call_target="tpu_custom_call" | custom-call | tf_op jit(solution)/shard_map/ffn_step/pallas_call | solution.py:578
  98.0 1.1 %ffn_store.1 = (bf16[128,2048]{1,0:T(8,128)(2,1)}, bf16[128,2048]{1,0:T(8,128)(2,1)}, f32[64,512]{1,0:T(8,128)}, f32[64,512]{1,0:T(8,128)}) custom-call(bf16[128,2048]{1,0:T(8,128)(2,1)S(1)} %get-tuple-element.8.refs_0_, bf16[128,2048]{1,0:T(8,128)(2,1)S(1)} %get-tuple-element.9.refs_1_, f32[64,512]{1,0:T(8,128)S(1)} %get-tuple-element.10.refs_2_, ...), custom_call_target="tpu_custom_call" | custom-call | tf_op jit(solution)/shard_map/ffn_store/pallas_call | solution.py:589

commit v3 on v2

--- a/solution.py
+++ b/solution.py
@@ -12,7 +12,7 @@
 BF = jnp.bfloat16
 F32 = jnp.float32
 N_SENT = 13
-N_GOT = 68
+N_GOT = 71
 
 
 def scratch_of(tok, d, ff, rows):
@@ -406,27 +406,79 @@
             out[k] = (total + other[k].astype(F32)).astype(BF)
 
     su, sd = r.su, r.sd
+
+    def z_sum(name, acc, plus, minus, size):
+        steps = {(s, first): group() for s in range(3) for first in (True, False)}
+        steps[3, True] = steps[3, False] = end = group()
+
+        def ways(s, first):
+            for k, buf, step in ((zi(4 - s), plus, 1), (zi(s - 4), minus, -1)):
+                yield k, buf, step, pl.ds(0 if first == (step == 1) else size, size)
+
+        def start(s, first):
+            for k, buf, step, part in ways(s, first):
+                send(acc.at[k, part], buf.at[s, part], dev(dz=step), steps[s, first])
+
+        def hop(s, first):
+            got(f"{name}{s}", steps[s - 1, first])
+            for k, buf, step, part in ways(s, first):
+                total = acc[k, part].astype(F32) + buf[s - 1, part].astype(F32)
+                acc[k, part] = total.astype(BF)
+            start(s, first)
+
+        def finish():
+            got(f"{name}4", end)
+            return acc[z].astype(F32) + plus[3].astype(F32) + minus[3].astype(F32)
+
+        return start, hop, finish
+
+    z_send, hop, z_end = z_sum("hop", sd, r.ra, r.rb, hz)
+    uz_send, uz_hop, uz_end = z_sum("uz", r.tu, r.ua, r.ub, rows // 2)
+
+    @jax.named_scope("back")
+    def back(left, weight, out, part):
+        @pl.loop(0, NZ // 2)
+        def _(k):
+            for core in range(2):
+                w = weight[core, pl.ds(2 * k, 2)].reshape(2 * per_z, ff)
+                acc = dot_tt(left[part, core * ff : (core + 1) * ff], w)
+                total = acc if core == 0 else total + acc
+            at = pl.ds(pl.multiple_of(k * 2 * per_z, per_z), 2 * per_z)
+            out[part, at] = total.astype(BF)
+
+    def start_sum(p, s):
+        g = group()
+        send(p.at[rows_of(3, 0)], s.at[0], dev(dy=1), g)
+        send(p.at[rows_of(3, 1)], s.at[1], dev(dy=-1), g)
+        return g
+
+    def more_sum(p, m):
+        g0, g1 = group(), group()
+        send(p.at[rows_of(2, 1)], m.at[0, pl.ds(half, half)], dev(dy=1), g1)
+        send(p.at[rows_of(1, 0)], m.at[1, pl.ds(0, half)], dev(dy=-1), g0)
+        return g0, g1
+
+    def pass_sum(p, s, m, g, groups):
+        g0, g1 = groups
+        got("sum_first", g)
+        at = rows_of(2, 0)
+        p[at] = (p[at].astype(F32) + s[0].astype(F32)).astype(BF)
+        send(p.at[at], m.at[0, pl.ds(0, half)], dev(dy=1), g0)
+        at = rows_of(1, 1)
+        p[at] = (p[at].astype(F32) + s[1].astype(F32)).astype(BF)
+        send(p.at[at], m.at[1, pl.ds(half, half)], dev(dy=-1), g1)
+
+    def end_sum(p, m, groups, out):
+        for h in range(2):
+            got("sum_end", groups[h])
+            own = rows_of(0, h)
+            total = p[own].astype(F32) + m[0, own].astype(F32) + m[1, own].astype(F32)
+            out[own] = total.astype(BF)
+
+    back(r.pg, wu, r.pe, last)
     c_down = cross_grad(r.ct, r.hid, r.god, r.xd, farthest)
-
-    arrived = {(s, first): group() for s in range(3) for first in (True, False)}
-    z_last = group()
-    for first in (True, False):
-        arrived[3, first] = z_last
-
-    def z_send(s, first):
-        g = arrived[s, first]
-        for k, buf, step in ((zi(4 - s), r.ra, 1), (zi(s - 4), r.rb, -1)):
-            part = pl.ds(0 if first == (step == 1) else hz, hz)
-            send(sd.at[k, part], buf.at[s, part], dev(dz=step), g)
-
-    def hop(s, first):
-        got(f"hop{s}", arrived[s - 1, first])
-        for k, buf, step in ((zi(4 - s), r.ra, 1), (zi(s - 4), r.rb, -1)):
-            part = pl.ds(0 if first == (step == 1) else hz, hz)
-            total = sd[k, part].astype(F32) + buf[s - 1, part].astype(F32)
-            sd[k, part] = total.astype(BF)
-        z_send(s, first)
-
+    pass_tokens(r.yl, l_a, tok_l)
+    first_e = start_sum(r.pe, r.se)
     c_up = cross_grad(r.et, r.pg, r.gou, r.xu, lambda j: j)
     for part in range(4):
         got("c_down", c_down[part])
@@ -435,8 +487,6 @@
             z_send(0, True)
         if part == 1:
             z_send(1, False)
-        if part == 2:
-            pass_tokens(r.yl, l_a, tok_l)
 
     nh = NZ // 2
     lo, hi = pl.ds(0, nh), pl.ds(nh, nh)
@@ -450,43 +500,8 @@
     send(su.at[hi, xs(1)], r.rx.at[0, hi], dev(dx=1), ur)
     send(su.at[lo, xs(-1)], r.rx.at[1, lo], dev(dx=-1), ur)
 
-    @jax.named_scope("back")
-    def back(left, weight, out):
-        @pl.loop(0, NZ // 2)
-        def _(k):
-            for core in range(2):
-                w = weight[core, pl.ds(2 * k, 2)].reshape(2 * per_z, ff)
-                acc = dot_tt(left[:, core * ff : (core + 1) * ff], w)
-                total = acc if core == 0 else total + acc
-            out[:, pl.ds(pl.multiple_of(k * 2 * per_z, per_z), 2 * per_z)] = total.astype(BF)
-
-    def start_sum(p, s, m):
-        g, g0, g1 = group(), group(), group()
-        send(p.at[rows_of(3, 0)], s.at[0], dev(dy=1), g)
-        send(p.at[rows_of(3, 1)], s.at[1], dev(dy=-1), g)
-        send(p.at[rows_of(2, 1)], m.at[0, pl.ds(half, half)], dev(dy=1), g1)
-        send(p.at[rows_of(1, 0)], m.at[1, pl.ds(0, half)], dev(dy=-1), g0)
-        return g, g0, g1
-
-    def pass_sum(p, s, m, groups):
-        g, g0, g1 = groups
-        got("sum_first", g)
-        at = rows_of(2, 0)
-        p[at] = (p[at].astype(F32) + s[0].astype(F32)).astype(BF)
-        send(p.at[at], m.at[0, pl.ds(0, half)], dev(dy=1), g0)
-        at = rows_of(1, 1)
-        p[at] = (p[at].astype(F32) + s[1].astype(F32)).astype(BF)
-        send(p.at[at], m.at[1, pl.ds(half, half)], dev(dy=-1), g1)
-
-    def end_sum(p, m, groups, out):
-        for h in range(2):
-            got("sum_end", groups[1 + h])
-            own = rows_of(0, h)
-            total = p[own].astype(F32) + m[0, own].astype(F32) + m[1, own].astype(F32)
-            out[own] = total.astype(BF)
-
-    back(r.pg, wu, r.pe)
-    y_e = start_sum(r.pe, r.se, r.re)
+    back(r.pg, wu, r.pe, many)
+    more_e = more_sum(r.pe, r.re)
     hop(1, True)
     hop(2, False)
 
@@ -501,13 +516,13 @@
     su[hi, xs(-1)] = (su[hi, xs(-1)].astype(F32) + r.sx[1].astype(F32)).astype(BF)
     send(su.at[hi, xs(-1)], r.rx.at[1, hi], dev(dx=-1), ur)
     hop(3, False)
-    back(r.hid, wd, r.po)
-    pass_sum(r.pe, r.se, r.re, y_e)
-    y_o = start_sum(r.po, r.so, r.ro)
+    pass_sum(r.pe, r.se, r.re, first_e, more_e)
+    back(r.hid, wd, r.po, pl.ds(0, 4 * tok))
+    first_o = start_sum(r.po, r.so)
+    more_o = more_sum(r.po, r.ro)
     hop(3, True)
 
-    got("hop4", z_last)
-    down_sum = sd[z].astype(F32) + r.ra[3].astype(F32) + r.rb[3].astype(F32)
+    down_sum = z_end()
     td = r.td
     td[...] = down_sum.astype(BF).reshape(NX, rows, ff)
     q0, q1 = pl.ds(0, rows // 2), pl.ds(rows // 2, rows // 2)
@@ -520,41 +535,32 @@
     tu[...] = (
         su[:, xs(0)].astype(F32) + r.rx[0].astype(F32) + r.rx[1].astype(F32)
     ).astype(BF)
-    uz = [group() for _ in range(4)]
-    send(tu.at[zi(4), q0], r.ua.at[0, q0], dev(dz=1), uz[0])
-    send(tu.at[zi(4), q1], r.ub.at[0, q1], dev(dz=-1), uz[0])
+    uz_send(0, True)
+    uz_send(1, False)
 
     def add_on(acc, k, buf, s, part):
         acc[k, part] = (acc[k, part].astype(F32) + buf[s, part].astype(F32)).astype(BF)
-
-    def up_hop(s):
-        got(f"uz{s}", uz[s - 1])
-        whole = pl.ds(0, rows)
-        add_on(tu, zi(4 - s), r.ua, s - 1, q0 if s == 1 else whole)
-        send(tu.at[zi(4 - s)], r.ua.at[s], dev(dz=1), uz[s])
-        add_on(tu, zi(s - 4), r.ub, s - 1, q1 if s == 1 else whole)
-        send(tu.at[zi(s - 4)], r.ub.at[s], dev(dz=-1), uz[s])
 
     got("dx1", dx1)
     add_on(td, xi(1), r.xa, 0, q0)
     send(td.at[xi(1)], r.xa.at[1], dev(dx=1), dx2)
     add_on(td, xi(-1), r.xb, 0, q1)
     send(td.at[xi(-1)], r.xb.at[1], dev(dx=-1), dx2)
-    up_hop(1)
+    uz_hop(1, True)
+    uz_hop(2, False)
     for copy in totals:
         copy.wait()
+    uz_hop(2, True)
+    uz_hop(3, False)
     got("dx2", dx2)
     total = td[x].astype(F32) + r.xa[1].astype(F32) + r.xb[1].astype(F32)
     o_down[...] = r.tot_d[...] + total * factor
-    up_hop(2)
-    pass_sum(r.po, r.so, r.ro, y_o)
-    up_hop(3)
-    end_sum(r.pe, r.re, y_e, o_earlier)
-    got("uz4", uz[3])
-    total = tu[z].astype(F32) + r.ua[3].astype(F32) + r.ub[3].astype(F32)
-    o_up[...] = r.tot_u[...] + total * factor
+    uz_hop(3, True)
+    pass_sum(r.po, r.so, r.ro, first_o, more_o)
+    end_sum(r.pe, r.re, more_e, o_earlier)
+    o_up[...] = r.tot_u[...] + uz_end() * factor
     settle()
-    end_sum(r.po, r.ro, y_o, o_later)
+    end_sum(r.po, r.ro, more_o, o_later)
     assert len(leaving) == N_SENT and len(arriving) == N_GOT, (len(leaving), len(arriving))
 
 

time: 99.2 us -> 96.6 us (0.974); the launches traced: 99.1 us -> 94.7 us
  Pallas kernels: 98.4 us -> 94.1 us
    pallas_call x1, Pallas kernels: 97.4 us -> 93 us  [body(): pl.pallas_call(run, out_shape=shapes, in_specs=[pl.BlockSpec(memory_space...]
where the time goes in v3:
time: 96.6 us; the launch traced here: 94.7 us
  Pallas kernels  94.1 us (97%)
    pallas_call x1, Pallas kernels, body(): pl.pallas_call(run, out_shape=shapes, in_specs=[pl.BlockSpec(memory_space...  93 us

profile of v3, /device:TPU:1, one launch (start us, length us, event | category | flops | bytes accessed | tf_op | source)
XLA Modules:
  0.0 94.7 jit_solution(12011932123291392490)
XLA Ops:
  0.6 93.0 %ffn_step.1 = (bf16[128,2048]{1,0:T(8,128)(2,1)S(1)}, bf16[128,2048]{1,0:T(8,128)(2,1)S(1)}, f32[64,512]{1,0:T(8,128)S(1)}, f32[64,512]{1,0:T(8,128)S(1)}) custom-call(bf16[128,2048]{1,0:T(8,128)(2,1)} %refs_0_.1, bf16[128,2048]{1,0:T(8,128)(2,1)} %refs_1_.1, bf16[128,2048]{1,0:T(8,128)(2,1)} %refs_2_.1, bf16[64,512]{1,0:T(8,128)(2,1)} %refs_3_.1, ...), custom_call_target="tpu_custom_call" | custom-call | tf_op jit(solution)/shard_map/ffn_step/pallas_call | solution.py:584
  93.6 1.1 %ffn_store.1 = (bf16[128,2048]{1,0:T(8,128)(2,1)}, bf16[128,2048]{1,0:T(8,128)(2,1)}, f32[64,512]{1,0:T(8,128)}, f32[64,512]{1,0:T(8,128)}) custom-call(bf16[128,2048]{1,0:T(8,128)(2,1)S(1)} %get-tuple-element.8.refs_0_, bf16[128,2048]{1,0:T(8,128)(2,1)S(1)} %get-tuple-element.9.refs_1_, f32[64,512]{1,0:T(8,128)S(1)} %get-tuple-element.10.refs_2_, ...), custom_call_target="tpu_custom_call" | custom-call | tf_op jit(solution)/shard_map/ffn_store/pallas_call | solution.py:595

commit v4 on v3

--- a/solution.py
+++ b/solution.py
@@ -12,7 +12,7 @@
 BF = jnp.bfloat16
 F32 = jnp.float32
 N_SENT = 13
-N_GOT = 71
+N_GOT = 67
 
 
 def scratch_of(tok, d, ff, rows):
@@ -55,7 +55,8 @@
         tot_d=vm((rows, ff), F32),
         send=pltpu.SemaphoreType.DMA((N_SENT,)),
         recv=pltpu.SemaphoreType.DMA((N_GOT,)),
-        local=pltpu.SemaphoreType.DMA((7,)),
+        told=pltpu.SemaphoreType.REGULAR,
+        local=pltpu.SemaphoreType.DMA((2,)),
     )
 
 
@@ -85,7 +86,7 @@
 
     def dev(dz=0, dx=0, dy=0, dc=0):
         fs = zi(dz) * NX + xi(dx)
-        tp = ((y + dy + NY) % NY) * 2 + (c + dc) % 2
+        tp = ((y + dy + NY) % NY) * 2 + (c + dc + 2) % 2
         return {"fs": fs, "tp": tp}
 
     row_bytes = d * 2
@@ -130,34 +131,68 @@
             for g in {g.at: g for g in groups}.values():
                 wait(r.recv.at[g.at], g)
 
-    local = []
-
-    def fetch(src, dst):
-        copy = pltpu.make_async_copy(src, dst, r.local.at[len(local)])
-        copy.start()
-        local.append(copy)
-        return copy
+    def fetch(i, *pairs):
+        g = SimpleNamespace(bytes=0)
+        for src, dst in pairs:
+            pltpu.make_async_copy(src, dst, r.local.at[i]).start()
+            g.bytes += math.prod(src.shape) * src.dtype.itemsize
+        return lambda: wait(r.local.at[i], g)
 
     def xs(k):
         return pl.ds(pl.multiple_of(xi(k) * rows, rows), rows)
 
-    first = [
-        fetch(earlier, r.ye.at[pl.ds(0, tok)]),
-        fetch(cot, r.yc.at[pl.ds(0, tok)]),
-        fetch(up, r.wu.at[0, z, xs(0)]),
-        fetch(down, r.wd.at[0, z, xs(0)]),
-        fetch(later, r.yl.at[pl.ds(0, tok)]),
-    ]
-    totals = [fetch(up_total, r.tot_u), fetch(down_total, r.tot_d)]
+    inputs = fetch(
+        0,
+        (earlier, r.ye.at[pl.ds(0, tok)]),
+        (up, r.wu.at[0, z, xs(0)]),
+        (down, r.wd.at[0, z, xs(0)]),
+        (cot, r.yc.at[pl.ds(0, tok)]),
+        (later, r.yl.at[pl.ds(0, tok)]),
+    )
+    totals = fetch(1, (up_total, r.tot_u), (down_total, r.tot_d))
 
     barrier = pltpu.get_barrier_semaphore()
-    partners = [dev(dy=1), dev(dy=-1), dev(dx=1), dev(dx=-1), dev(dz=1), dev(dz=-1), dev(dc=1)]
-    for p in partners:
-        pl.semaphore_signal(barrier, inc=1, device_id=p, device_id_type=pl.DeviceIdType.MESH)
+
+    def enter(**to):
+        pl.semaphore_signal(
+            barrier, inc=1, device_id=dev(**to), device_id_type=pl.DeviceIdType.MESH
+        )
+
+    def tell():
+        pl.semaphore_signal(
+            r.told, inc=1, device_id=dev(dc=1), device_id_type=pl.DeviceIdType.MESH
+        )
+
+    for step in (1, -1):
+        enter(dy=step, dc=-c)
+        enter(dx=step, dc=-c)
+        enter(dz=step, dc=1 - c)
+    enter(dc=1)
+
     with jax.named_scope("barrier"):
-        pl.semaphore_wait(barrier, len(partners))
-        for copy in first:
-            copy.wait()
+
+        @pl.when(c == 0)
+        def _():
+            pl.semaphore_wait(barrier, 9)
+            tell()
+
+        @pl.when(c == 1)
+        def _():
+            pl.semaphore_wait(r.told, 1)
+
+        inputs()
+
+    def enter_z():
+        with jax.named_scope("barrier_z"):
+
+            @pl.when(c == 1)
+            def _():
+                pl.semaphore_wait(barrier, 5)
+                tell()
+
+            @pl.when(c == 0)
+            def _():
+                pl.semaphore_wait(r.told, 1)
 
     def rows_of(slot, h):
         return pl.ds(slot * tok + h * half, half)
@@ -189,18 +224,18 @@
             send(ref, ref, dev(dz=step), g)
         return g
 
-    up_first, up_rest, up_last = {}, group(), group()
+    up_first, up_rest, up_last = [group() for _ in range(4)], group(), group()
 
     def up_to_x(dz):
         ref = up_block(dz, 0)
-        up_first[dz] = group()
-        plus, minus = (up_first[dz], up_rest) if 0 <= dz <= 3 else (up_rest, up_first[dz])
+        first = up_first[min(abs(dz), 3)]
+        plus, minus = (first, up_rest) if 0 <= dz <= 3 else (up_rest, first)
         send(ref, ref, dev(dx=1), plus)
         send(ref, ref, dev(dx=-1), minus)
 
     def up_pass_x(*dzs):
+        got("up_x", up_first[min(abs(dzs[0]), 3)])
         for dz in dzs:
-            got("up_x", up_first[dz])
             step = 1 if 0 <= dz <= 3 else -1
             ref = up_block(dz, -step)
             send(ref, ref, dev(dx=step), up_last)
@@ -245,16 +280,17 @@
             dst[cols, pl.ds(slot * tok, tok)] = src[pl.ds(slot * tok, tok), cols].T
 
     e_a = own_tokens(r.ye, 0)
-    up_1 = up_z(0)
     own_down = down_block(0, 0)
     down_x1, down_x2 = group(), group()
     send(own_down, own_down, dev(dx=1), down_x1)
     send(own_down, own_down, dev(dx=-1), down_x1)
-    down_z(0, 0)
     up_to_x(0)
     c_a = own_tokens(r.yc, 0)
     tok_own = own_tokens(r.ye, 1)
     own_tokens(r.yc, 1, tok_own)
+    enter_z()
+    up_1 = up_z(0)
+    down_z(0, 0)
     turn(0, r.ye, r.et)
 
     got("up_z1", up_1)
@@ -393,10 +429,9 @@
             ks = order(2 * part), order(2 * part + 1)
             for k, total in zip(ks, gradient(left, right, ks, 1)):
                 out[k] = total.astype(BF)
-            g = group()
+            copies.append(group())
             for k in ks:
-                send(out.at[k], into.at[k], dev(dc=1), g)
-            copies.append(g)
+                send(out.at[k], into.at[k], dev(dc=1), copies[-1])
         return copies
 
     @jax.named_scope("own_grad")
@@ -476,9 +511,9 @@
             out[own] = total.astype(BF)
 
     back(r.pg, wu, r.pe, last)
-    c_down = cross_grad(r.ct, r.hid, r.god, r.xd, farthest)
     pass_tokens(r.yl, l_a, tok_l)
     first_e = start_sum(r.pe, r.se)
+    c_down = cross_grad(r.ct, r.hid, r.god, r.xd, farthest)
     c_up = cross_grad(r.et, r.pg, r.gou, r.xu, lambda j: j)
     for part in range(4):
         got("c_down", c_down[part])
@@ -511,12 +546,12 @@
     su[lo, xs(1)] = (su[lo, xs(1)].astype(F32) + r.sx[0].astype(F32)).astype(BF)
     send(su.at[lo, xs(1)], r.rx.at[0, lo], dev(dx=1), ur)
     hop(2, True)
+    pass_sum(r.pe, r.se, r.re, first_e, more_e)
     pre_later(1)
     got("ux", ux_b)
     su[hi, xs(-1)] = (su[hi, xs(-1)].astype(F32) + r.sx[1].astype(F32)).astype(BF)
     send(su.at[hi, xs(-1)], r.rx.at[1, hi], dev(dx=-1), ur)
     hop(3, False)
-    pass_sum(r.pe, r.se, r.re, first_e, more_e)
     back(r.hid, wd, r.po, pl.ds(0, 4 * tok))
     first_o = start_sum(r.po, r.so)
     more_o = more_sum(r.po, r.ro)
@@ -548,15 +583,14 @@
     send(td.at[xi(-1)], r.xb.at[1], dev(dx=-1), dx2)
     uz_hop(1, True)
     uz_hop(2, False)
-    for copy in totals:
-        copy.wait()
+    totals()
     uz_hop(2, True)
+    pass_sum(r.po, r.so, r.ro, first_o, more_o)
     uz_hop(3, False)
     got("dx2", dx2)
     total = td[x].astype(F32) + r.xa[1].astype(F32) + r.xb[1].astype(F32)
     o_down[...] = r.tot_d[...] + total * factor
     uz_hop(3, True)
-    pass_sum(r.po, r.so, r.ro, first_o, more_o)
     end_sum(r.pe, r.re, more_e, o_earlier)
     o_up[...] = r.tot_u[...] + uz_end() * factor
     settle()

time: 96.6 us -> 94.5 us (0.978); the launches traced: 94.7 us -> 93.9 us
  no operation moved by 1% of the time
where the time goes in v4:
time: 94.5 us; the launch traced here: 93.9 us
  Pallas kernels  93.3 us (99%)
    pallas_call x1, Pallas kernels, body(): pl.pallas_call(run, out_shape=shapes, in_specs=[pl.BlockSpec(memory_space...  92.2 us

profile of v4, /device:TPU:1, one launch (start us, length us, event | category | flops | bytes accessed | tf_op | source)
XLA Modules:
  0.0 93.9 jit_solution(11216759210541454271)
XLA Ops:
  0.6 92.2 %ffn_step.1 = (bf16[128,2048]{1,0:T(8,128)(2,1)S(1)}, bf16[128,2048]{1,0:T(8,128)(2,1)S(1)}, f32[64,512]{1,0:T(8,128)S(1)}, f32[64,512]{1,0:T(8,128)S(1)}) custom-call(bf16[128,2048]{1,0:T(8,128)(2,1)} %refs_0_.1, bf16[128,2048]{1,0:T(8,128)(2,1)} %refs_1_.1, bf16[128,2048]{1,0:T(8,128)(2,1)} %refs_2_.1, bf16[64,512]{1,0:T(8,128)(2,1)} %refs_3_.1, ...), custom_call_target="tpu_custom_call" | custom-call | tf_op jit(solution)/shard_map/ffn_step/pallas_call | solution.py:618
  92.9 1.1 %ffn_store.1 = (bf16[128,2048]{1,0:T(8,128)(2,1)}, bf16[128,2048]{1,0:T(8,128)(2,1)}, f32[64,512]{1,0:T(8,128)}, f32[64,512]{1,0:T(8,128)}) custom-call(bf16[128,2048]{1,0:T(8,128)(2,1)S(1)} %get-tuple-element.8.refs_0_, bf16[128,2048]{1,0:T(8,128)(2,1)S(1)} %get-tuple-element.9.refs_1_, f32[64,512]{1,0:T(8,128)S(1)} %get-tuple-element.10.refs_2_, ...), custom_call_target="tpu_custom_call" | custom-call | tf_op jit(solution)/shard_map/ffn_store/pallas_call | solution.py:629

commit v5 on v4

--- a/solution.py
+++ b/solution.py
@@ -12,7 +12,7 @@
 BF = jnp.bfloat16
 F32 = jnp.float32
 N_SENT = 13
-N_GOT = 67
+N_GOT = 72
 
 
 def scratch_of(tok, d, ff, rows):
@@ -39,7 +39,7 @@
         xd=vm((NZ, per_z, ff), BF),
         su=vm((NZ, per_z, ff), BF),
         sd=vm((NZ, per_z, ff), BF),
-        sx=vm((2, NZ // 2, rows, ff), BF),
+        sx=vm((NZ // 2, 2, rows, ff), BF),
         rx=vm((2, NZ, rows, ff), BF),
         tu=vm((NZ, rows, ff), BF),
         ua=vm((4, rows, ff), BF),
@@ -165,7 +165,7 @@
 
     for step in (1, -1):
         enter(dy=step, dc=-c)
-        enter(dx=step, dc=-c)
+        enter(dx=step, dc=1 - c)
         enter(dz=step, dc=1 - c)
     enter(dc=1)
 
@@ -173,7 +173,7 @@
 
         @pl.when(c == 0)
         def _():
-            pl.semaphore_wait(barrier, 9)
+            pl.semaphore_wait(barrier, 5)
             tell()
 
         @pl.when(c == 1)
@@ -182,12 +182,12 @@
 
         inputs()
 
-    def enter_z():
-        with jax.named_scope("barrier_z"):
+    def enter_xz():
+        with jax.named_scope("barrier_xz"):
 
             @pl.when(c == 1)
             def _():
-                pl.semaphore_wait(barrier, 5)
+                pl.semaphore_wait(barrier, 9)
                 tell()
 
             @pl.when(c == 0)
@@ -280,15 +280,15 @@
             dst[cols, pl.ds(slot * tok, tok)] = src[pl.ds(slot * tok, tok), cols].T
 
     e_a = own_tokens(r.ye, 0)
+    c_a = own_tokens(r.yc, 0)
+    tok_own = own_tokens(r.ye, 1)
+    own_tokens(r.yc, 1, tok_own)
+    enter_xz()
     own_down = down_block(0, 0)
     down_x1, down_x2 = group(), group()
     send(own_down, own_down, dev(dx=1), down_x1)
     send(own_down, own_down, dev(dx=-1), down_x1)
     up_to_x(0)
-    c_a = own_tokens(r.yc, 0)
-    tok_own = own_tokens(r.ye, 1)
-    own_tokens(r.yc, 1, tok_own)
-    enter_z()
     up_1 = up_z(0)
     down_z(0, 0)
     turn(0, r.ye, r.et)
@@ -471,8 +471,8 @@
     uz_send, uz_hop, uz_end = z_sum("uz", r.tu, r.ua, r.ub, rows // 2)
 
     @jax.named_scope("back")
-    def back(left, weight, out, part):
-        @pl.loop(0, NZ // 2)
+    def back(left, weight, out, part, begin=0, end=NZ // 2):
+        @pl.loop(begin, end)
         def _(k):
             for core in range(2):
                 w = weight[core, pl.ds(2 * k, 2)].reshape(2 * per_z, ff)
@@ -510,11 +510,13 @@
             total = p[own].astype(F32) + m[0, own].astype(F32) + m[1, own].astype(F32)
             out[own] = total.astype(BF)
 
-    back(r.pg, wu, r.pe, last)
+    back(r.pg, wu, r.pe, last, end=NZ // 4)
     pass_tokens(r.yl, l_a, tok_l)
+    back(r.pg, wu, r.pe, last, begin=NZ // 4)
     first_e = start_sum(r.pe, r.se)
     c_down = cross_grad(r.ct, r.hid, r.god, r.xd, farthest)
-    c_up = cross_grad(r.et, r.pg, r.gou, r.xu, lambda j: j)
+    pairs = ((4, 0), (3, 5), (2, 6), (1, 7))
+    c_up = cross_grad(r.et, r.pg, r.gou, r.xu, lambda j: zi(pairs[j // 2][j % 2]))
     for part in range(4):
         got("c_down", c_down[part])
         own_grad(r.ct, r.hid, r.xd, sd, farthest, part)
@@ -523,39 +525,65 @@
         if part == 1:
             z_send(1, False)
 
-    nh = NZ // 2
-    lo, hi = pl.ds(0, nh), pl.ds(nh, nh)
-    ux_a, ux_b, ur = group(), group(), group()
+    x_first, x_last = [group() for _ in pairs], [group() for _ in pairs]
+
+    def x_send(p):
+        for i, step in ((0, 1), (1, -1)):
+            k = zi(pairs[p][i])
+            send(su.at[k, xs(2)], r.sx.at[p, i], dev(dx=step), x_first[p])
+
+    def x_hop(p):
+        got(f"x_hop{p}", x_first[p])
+        for i, step in ((0, 1), (1, -1)):
+            k = zi(pairs[p][i])
+            total = su[k, xs(step)].astype(F32) + r.sx[p, i].astype(F32)
+            su[k, xs(step)] = total.astype(BF)
+            send(su.at[k, xs(step)], r.rx.at[i, 2 * p + i], dev(dx=step), x_last[p])
+        for i, step in ((0, 1), (1, -1)):
+            k = zi(pairs[p][1 - i])
+            send(su.at[k, xs(step)], r.rx.at[i, 2 * p + 1 - i], dev(dx=step), x_last[p])
+
+    def x_end(p):
+        got(f"x_end{p}", x_last[p])
+        for i in range(2):
+            k, j = zi(pairs[p][i]), 2 * p + i
+            total = su[k, xs(0)].astype(F32) + r.rx[0, j].astype(F32) + r.rx[1, j].astype(F32)
+            r.tu[k] = total.astype(BF)
+
     for part in range(4):
         got("c_up", c_up[part])
-        own_grad(r.et, r.pg, r.xu, su, lambda j: j, part)
-        if part == 1:
-            send(su.at[lo, xs(2)], r.sx.at[0], dev(dx=1), ux_a)
-    send(su.at[hi, xs(2)], r.sx.at[1], dev(dx=-1), ux_b)
-    send(su.at[hi, xs(1)], r.rx.at[0, hi], dev(dx=1), ur)
-    send(su.at[lo, xs(-1)], r.rx.at[1, lo], dev(dx=-1), ur)
+        own_grad(r.et, r.pg, r.xu, su, lambda j: zi(pairs[j // 2][j % 2]), part)
+        x_send(part)
 
     back(r.pg, wu, r.pe, many)
     more_e = more_sum(r.pe, r.re)
     hop(1, True)
+    x_hop(0)
     hop(2, False)
 
     got("tok_l", tok_l)
     pre_later(0)
-    got("ux", ux_a)
-    su[lo, xs(1)] = (su[lo, xs(1)].astype(F32) + r.sx[0].astype(F32)).astype(BF)
-    send(su.at[lo, xs(1)], r.rx.at[0, lo], dev(dx=1), ur)
-    hop(2, True)
+    x_hop(1)
+    x_hop(2)
+    x_hop(3)
     pass_sum(r.pe, r.se, r.re, first_e, more_e)
     pre_later(1)
-    got("ux", ux_b)
-    su[hi, xs(-1)] = (su[hi, xs(-1)].astype(F32) + r.sx[1].astype(F32)).astype(BF)
-    send(su.at[hi, xs(-1)], r.rx.at[1, hi], dev(dx=-1), ur)
-    hop(3, False)
+    hop(2, True)
     back(r.hid, wd, r.po, pl.ds(0, 4 * tok))
     first_o = start_sum(r.po, r.so)
     more_o = more_sum(r.po, r.ro)
+    x_end(0)
+    uz_send(0, True)
+    hop(3, False)
+    x_end(1)
+    uz_send(1, False)
+    uz_hop(1, True)
     hop(3, True)
+    x_end(2)
+    uz_hop(2, False)
+    x_end(3)
+    uz_hop(2, True)
+    uz_hop(3, False)
 
     down_sum = z_end()
     td = r.td
@@ -564,35 +592,23 @@
     dx1, dx2 = group(), group()
     send(td.at[xi(2), q0], r.xa.at[0, q0], dev(dx=1), dx1)
     send(td.at[xi(2), q1], r.xb.at[0, q1], dev(dx=-1), dx1)
-
-    got("ur", ur)
-    tu = r.tu
-    tu[...] = (
-        su[:, xs(0)].astype(F32) + r.rx[0].astype(F32) + r.rx[1].astype(F32)
-    ).astype(BF)
-    uz_send(0, True)
-    uz_send(1, False)
+    uz_hop(3, True)
 
     def add_on(acc, k, buf, s, part):
         acc[k, part] = (acc[k, part].astype(F32) + buf[s, part].astype(F32)).astype(BF)
 
+    pass_sum(r.po, r.so, r.ro, first_o, more_o)
     got("dx1", dx1)
     add_on(td, xi(1), r.xa, 0, q0)
     send(td.at[xi(1)], r.xa.at[1], dev(dx=1), dx2)
     add_on(td, xi(-1), r.xb, 0, q1)
     send(td.at[xi(-1)], r.xb.at[1], dev(dx=-1), dx2)
-    uz_hop(1, True)
-    uz_hop(2, False)
     totals()
-    uz_hop(2, True)
-    pass_sum(r.po, r.so, r.ro, first_o, more_o)
-    uz_hop(3, False)
+    o_up[...] = r.tot_u[...] + uz_end() * factor
     got("dx2", dx2)
     total = td[x].astype(F32) + r.xa[1].astype(F32) + r.xb[1].astype(F32)
     o_down[...] = r.tot_d[...] + total * factor
-    uz_hop(3, True)
     end_sum(r.pe, r.re, more_e, o_earlier)
-    o_up[...] = r.tot_u[...] + uz_end() * factor
     settle()
     end_sum(r.po, r.ro, more_o, o_later)
     assert len(leaving) == N_SENT and len(arriving) == N_GOT, (len(leaving), len(arriving))

time: 94.5 us -> 94.3 us (level)
  no operation moved by 1% of the time
where the time goes in v5:
time: 94.3 us; the launch traced here: 94.2 us
  Pallas kernels  93.5 us (99%)
    pallas_call x1, Pallas kernels, body(): pl.pallas_call(run, out_shape=shapes, in_specs=[pl.BlockSpec(memory_space...  92.4 us

profile of v5, /device:TPU:1, one launch (start us, length us, event | category | flops | bytes accessed | tf_op | source)
XLA Modules:
  0.0 94.2 jit_solution(12307342300434276557)
XLA Ops:
  0.6 92.4 %ffn_step.1 = (bf16[128,2048]{1,0:T(8,128)(2,1)S(1)}, bf16[128,2048]{1,0:T(8,128)(2,1)S(1)}, f32[64,512]{1,0:T(8,128)S(1)}, f32[64,512]{1,0:T(8,128)S(1)}) custom-call(bf16[128,2048]{1,0:T(8,128)(2,1)} %refs_0_.1, bf16[128,2048]{1,0:T(8,128)(2,1)} %refs_1_.1, bf16[128,2048]{1,0:T(8,128)(2,1)} %refs_2_.1, bf16[64,512]{1,0:T(8,128)(2,1)} %refs_3_.1, ...), custom_call_target="tpu_custom_call" | custom-call | tf_op jit(solution)/shard_map/ffn_step/pallas_call | solution.py:634
  93.1 1.1 %ffn_store.1 = (bf16[128,2048]{1,0:T(8,128)(2,1)}, bf16[128,2048]{1,0:T(8,128)(2,1)}, f32[64,512]{1,0:T(8,128)}, f32[64,512]{1,0:T(8,128)}) custom-call(bf16[128,2048]{1,0:T(8,128)(2,1)S(1)} %get-tuple-element.8.refs_0_, bf16[128,2048]{1,0:T(8,128)(2,1)S(1)} %get-tuple-element.9.refs_1_, f32[64,512]{1,0:T(8,128)S(1)} %get-tuple-element.10.refs_2_, ...), custom_call_target="tpu_custom_call" | custom-call | tf_op jit(solution)/shard_map/ffn_store/pallas_call | solution.py:645

commit v6 on v5

--- a/solution.py
+++ b/solution.py
@@ -56,7 +56,7 @@
         send=pltpu.SemaphoreType.DMA((N_SENT,)),
         recv=pltpu.SemaphoreType.DMA((N_GOT,)),
         told=pltpu.SemaphoreType.REGULAR,
-        local=pltpu.SemaphoreType.DMA((2,)),
+        local=pltpu.SemaphoreType.DMA((4,)),
     )
 
 
@@ -141,16 +141,6 @@
     def xs(k):
         return pl.ds(pl.multiple_of(xi(k) * rows, rows), rows)
 
-    inputs = fetch(
-        0,
-        (earlier, r.ye.at[pl.ds(0, tok)]),
-        (up, r.wu.at[0, z, xs(0)]),
-        (down, r.wd.at[0, z, xs(0)]),
-        (cot, r.yc.at[pl.ds(0, tok)]),
-        (later, r.yl.at[pl.ds(0, tok)]),
-    )
-    totals = fetch(1, (up_total, r.tot_u), (down_total, r.tot_d))
-
     barrier = pltpu.get_barrier_semaphore()
 
     def enter(**to):
@@ -169,6 +159,16 @@
         enter(dz=step, dc=1 - c)
     enter(dc=1)
 
+    first = fetch(0, (earlier, r.ye.at[pl.ds(0, tok)]))
+    second = fetch(1, (cot, r.yc.at[pl.ds(0, tok)]))
+    inputs = fetch(
+        2,
+        (up, r.wu.at[0, z, xs(0)]),
+        (down, r.wd.at[0, z, xs(0)]),
+        (later, r.yl.at[pl.ds(0, tok)]),
+    )
+    totals = fetch(3, (up_total, r.tot_u), (down_total, r.tot_d))
+
     with jax.named_scope("barrier"):
 
         @pl.when(c == 0)
@@ -179,8 +179,6 @@
         @pl.when(c == 1)
         def _():
             pl.semaphore_wait(r.told, 1)
-
-        inputs()
 
     def enter_xz():
         with jax.named_scope("barrier_xz"):
@@ -279,10 +277,13 @@
             cols = pl.ds(pl.multiple_of(k * per_z, per_z), per_z)
             dst[cols, pl.ds(slot * tok, tok)] = src[pl.ds(slot * tok, tok), cols].T
 
+    first()
     e_a = own_tokens(r.ye, 0)
+    second()
     c_a = own_tokens(r.yc, 0)
     tok_own = own_tokens(r.ye, 1)
     own_tokens(r.yc, 1, tok_own)
+    inputs()
     enter_xz()
     own_down = down_block(0, 0)
     down_x1, down_x2 = group(), group()
@@ -510,9 +511,8 @@
             total = p[own].astype(F32) + m[0, own].astype(F32) + m[1, own].astype(F32)
             out[own] = total.astype(BF)
 
-    back(r.pg, wu, r.pe, last, end=NZ // 4)
     pass_tokens(r.yl, l_a, tok_l)
-    back(r.pg, wu, r.pe, last, begin=NZ // 4)
+    back(r.pg, wu, r.pe, last)
     first_e = start_sum(r.pe, r.se)
     c_down = cross_grad(r.ct, r.hid, r.god, r.xd, farthest)
     pairs = ((4, 0), (3, 5), (2, 6), (1, 7))

time: 94.3 us -> 93.5 us (level)
  no operation moved by 1% of the time
where the time goes in v6:
time: 93.5 us; the launch traced here: 93.4 us
  Pallas kernels  92.8 us (99%)
    pallas_call x1, Pallas kernels, body(): pl.pallas_call(run, out_shape=shapes, in_specs=[pl.BlockSpec(memory_space...  91.7 us

profile of v6, /device:TPU:1, one launch (start us, length us, event | category | flops | bytes accessed | tf_op | source)
XLA Modules:
  0.0 93.4 jit_solution(14266432138262148962)
XLA Ops:
  0.6 91.7 %ffn_step.1 = (bf16[128,2048]{1,0:T(8,128)(2,1)S(1)}, bf16[128,2048]{1,0:T(8,128)(2,1)S(1)}, f32[64,512]{1,0:T(8,128)S(1)}, f32[64,512]{1,0:T(8,128)S(1)}) custom-call(bf16[128,2048]{1,0:T(8,128)(2,1)} %refs_0_.1, bf16[128,2048]{1,0:T(8,128)(2,1)} %refs_1_.1, bf16[128,2048]{1,0:T(8,128)(2,1)} %refs_2_.1, bf16[64,512]{1,0:T(8,128)(2,1)} %refs_3_.1, ...), custom_call_target="tpu_custom_call" | custom-call | tf_op jit(solution)/shard_map/ffn_step/pallas_call | solution.py:634
  92.3 1.1 %ffn_store.1 = (bf16[128,2048]{1,0:T(8,128)(2,1)}, bf16[128,2048]{1,0:T(8,128)(2,1)}, f32[64,512]{1,0:T(8,128)}, f32[64,512]{1,0:T(8,128)}) custom-call(bf16[128,2048]{1,0:T(8,128)(2,1)S(1)} %get-tuple-element.8.refs_0_, bf16[128,2048]{1,0:T(8,128)(2,1)S(1)} %get-tuple-element.9.refs_1_, f32[64,512]{1,0:T(8,128)S(1)} %get-tuple-element.10.refs_2_, ...), custom_call_target="tpu_custom_call" | custom-call | tf_op jit(solution)/shard_map/ffn_store/pallas_call | solution.py:645

commit v7 on v6

--- a/solution.py
+++ b/solution.py
@@ -11,17 +11,15 @@
 NZ, NX, NY = 8, 4, 4
 BF = jnp.bfloat16
 F32 = jnp.float32
-N_SENT = 13
-N_GOT = 72
+N_SENT = 4
+N_GOT = 52
 
 
 def scratch_of(tok, d, ff, rows):
     per_z = NX * rows
     vm = pltpu.VMEM
     return dict(
-        ye=vm((4 * tok, d), BF),
-        yc=vm((4 * tok, d), BF),
-        yl=vm((4 * tok, d), BF),
+        tok=vm((12 * tok, d), BF),
         wu=vm((2, NZ, per_z, ff), BF),
         wd=vm((2, NZ, per_z, ff), BF),
         hid=vm((4 * tok, 2 * ff), BF),
@@ -70,6 +68,7 @@
     r = SimpleNamespace(**dict(zip(names, refs[11:])))
     tok, d = later.shape
     rows, ff = up.shape
+    r.ye, r.yc, r.yl = (r.tok.at[pl.ds(i * 4 * tok, 4 * tok)] for i in range(3))
     half = tok // 2
     per_z = NX * rows
     hz = per_z // 2
@@ -90,16 +89,18 @@
         return {"fs": fs, "tp": tp}
 
     row_bytes = d * 2
-    limit = r.ye.shape[0] * row_bytes
-    leaving, arriving = [], []
+    limit = r.tok.shape[0] * row_bytes
+    leaving, arriving, spent = [], [], []
 
     def group():
+        if spent:
+            return SimpleNamespace(at=spent.pop(), bytes=0)
         g = SimpleNamespace(at=len(arriving), bytes=0)
         arriving.append(g)
         return g
 
     def wait(sem, g):
-        ref = r.ye.at[pl.ds(0, g.bytes // row_bytes)]
+        ref = r.tok.at[pl.ds(0, g.bytes // row_bytes)]
         pltpu.make_async_copy(ref, ref, sem).wait()
 
     def send(src, dst, to, g=None):
@@ -126,10 +127,13 @@
                 wait(r.send.at[i], g)
                 g.done = True
 
+    done = []
+
     def got(name, *groups):
         with jax.named_scope(name):
             for g in {g.at: g for g in groups}.values():
                 wait(r.recv.at[g.at], g)
+                done.append(g.at)
 
     def fetch(i, *pairs):
         g = SimpleNamespace(bytes=0)
@@ -238,11 +242,11 @@
             ref = up_block(dz, -step)
             send(ref, ref, dev(dx=step), up_last)
 
-    across_up, across_down = group(), group()
+    across = group()
 
     def up_column(dx):
         src = wu.at[0, :, xs(dx)]
-        send(src, wu.at[1, :, xs(dx)], dev(dc=1), across_up)
+        send(src, wu.at[1, :, xs(dx)], dev(dc=1), across)
 
     def down_block(dz, dx):
         return wd.at[0, zi(dz), xs(dx)]
@@ -268,7 +272,7 @@
 
     def down_chunk(*dzs):
         for dz in dzs:
-            send(wd.at[0, zi(dz)], wd.at[1, zi(dz)], dev(dc=1), across_down)
+            send(wd.at[0, zi(dz)], wd.at[1, zi(dz)], dev(dc=1), across)
 
     @jax.named_scope("turn")
     def turn(slot, src, dst):
@@ -329,6 +333,7 @@
     up_to_x(4)
     up_column(0)
     c_f = pass_tokens(r.yc, c_a)
+    free = list(done)
     l_a = own_tokens(r.yl, 0)
     tok_l = own_tokens(r.yl, 1)
     up_pass_x(-2, 2)
@@ -350,7 +355,8 @@
     for slot in (1, 2):
         turn(slot, r.ye, r.et)
         turn(slot, r.yc, r.ct)
-    got("across", across_up, across_down)
+    got("across", across)
+    spent += free
 
     tile = 256
     many, last = pl.ds(0, 3 * tok), pl.ds(3 * tok, tok)
@@ -444,7 +450,8 @@
     su, sd = r.su, r.sd
 
     def z_sum(name, acc, plus, minus, size):
-        steps = {(s, first): group() for s in range(3) for first in (True, False)}
+        order = (0, True), (1, True), (1, False), (2, True), (2, False)
+        steps = {key: group() for key in order}
         steps[3, True] = steps[3, False] = end = group()
 
         def ways(s, first):

time: 93.5 us -> 93.3 us (level)
  no operation moved by 1% of the time
where the time goes in v7:
time: 93.3 us; the launch traced here: 93.1 us
  Pallas kernels  92.5 us (99%)
    pallas_call x1, Pallas kernels, body(): pl.pallas_call(run, out_shape=shapes, in_specs=[pl.BlockSpec(memory_space...  91.4 us

profile of v7, /device:TPU:1, one launch (start us, length us, event | category | flops | bytes accessed | tf_op | source)
XLA Modules:
  0.0 93.1 jit_solution(1423439157964039974)
XLA Ops:
  0.6 91.4 %ffn_step.1 = (bf16[128,2048]{1,0:T(8,128)(2,1)S(1)}, bf16[128,2048]{1,0:T(8,128)(2,1)S(1)}, f32[64,512]{1,0:T(8,128)S(1)}, f32[64,512]{1,0:T(8,128)S(1)}) custom-call(bf16[128,2048]{1,0:T(8,128)(2,1)} %refs_0_.1, bf16[128,2048]{1,0:T(8,128)(2,1)} %refs_1_.1, bf16[128,2048]{1,0:T(8,128)(2,1)} %refs_2_.1, bf16[64,512]{1,0:T(8,128)(2,1)} %refs_3_.1, ...), custom_call_target="tpu_custom_call" | custom-call | tf_op jit(solution)/shard_map/ffn_step/pallas_call | solution.py:641
  92.1 1.1 %ffn_store.1 = (bf16[128,2048]{1,0:T(8,128)(2,1)}, bf16[128,2048]{1,0:T(8,128)(2,1)}, f32[64,512]{1,0:T(8,128)}, f32[64,512]{1,0:T(8,128)}) custom-call(bf16[128,2048]{1,0:T(8,128)(2,1)S(1)} %get-tuple-element.8.refs_0_, bf16[128,2048]{1,0:T(8,128)(2,1)S(1)} %get-tuple-element.9.refs_1_, f32[64,512]{1,0:T(8,128)S(1)} %get-tuple-element.10.refs_2_, ...), custom_call_target="tpu_custom_call" | custom-call | tf_op jit(solution)/shard_map/ffn_store/pallas_call | solution.py:652

commit v8 on v7

--- a/solution.py
+++ b/solution.py
@@ -54,7 +54,7 @@
         send=pltpu.SemaphoreType.DMA((N_SENT,)),
         recv=pltpu.SemaphoreType.DMA((N_GOT,)),
         told=pltpu.SemaphoreType.REGULAR,
-        local=pltpu.SemaphoreType.DMA((4,)),
+        local=pltpu.SemaphoreType.DMA((3,)),
     )
 
 
@@ -164,14 +164,14 @@
     enter(dc=1)
 
     first = fetch(0, (earlier, r.ye.at[pl.ds(0, tok)]))
-    second = fetch(1, (cot, r.yc.at[pl.ds(0, tok)]))
     inputs = fetch(
-        2,
+        1,
+        (cot, r.yc.at[pl.ds(0, tok)]),
         (up, r.wu.at[0, z, xs(0)]),
         (down, r.wd.at[0, z, xs(0)]),
         (later, r.yl.at[pl.ds(0, tok)]),
     )
-    totals = fetch(3, (up_total, r.tot_u), (down_total, r.tot_d))
+    totals = fetch(2, (up_total, r.tot_u), (down_total, r.tot_d))
 
     with jax.named_scope("barrier"):
 
@@ -283,11 +283,10 @@
 
     first()
     e_a = own_tokens(r.ye, 0)
-    second()
+    inputs()
     c_a = own_tokens(r.yc, 0)
     tok_own = own_tokens(r.ye, 1)
     own_tokens(r.yc, 1, tok_own)
-    inputs()
     enter_xz()
     own_down = down_block(0, 0)
     down_x1, down_x2 = group(), group()

time: 93.3 us -> 93.2 us (level)
  no operation moved by 1% of the time
where the time goes in v8:
time: 93.2 us; the launch traced here: 93.1 us
  Pallas kernels  92.5 us (99%)
    pallas_call x1, Pallas kernels, body(): pl.pallas_call(run, out_shape=shapes, in_specs=[pl.BlockSpec(memory_space...  91.4 us

profile of v8, /device:TPU:1, one launch (start us, length us, event | category | flops | bytes accessed | tf_op | source)
XLA Modules:
  0.0 93.1 jit_solution(11580087539467482847)
XLA Ops:
  0.6 91.4 %ffn_step.1 = (bf16[128,2048]{1,0:T(8,128)(2,1)S(1)}, bf16[128,2048]{1,0:T(8,128)(2,1)S(1)}, f32[64,512]{1,0:T(8,128)S(1)}, f32[64,512]{1,0:T(8,128)S(1)}) custom-call(bf16[128,2048]{1,0:T(8,128)(2,1)} %refs_0_.1, bf16[128,2048]{1,0:T(8,128)(2,1)} %refs_1_.1, bf16[128,2048]{1,0:T(8,128)(2,1)} %refs_2_.1, bf16[64,512]{1,0:T(8,128)(2,1)} %refs_3_.1, ...), custom_call_target="tpu_custom_call" | custom-call | tf_op jit(solution)/shard_map/ffn_step/pallas_call | solution.py:640
  92.1 1.1 %ffn_store.1 = (bf16[128,2048]{1,0:T(8,128)(2,1)}, bf16[128,2048]{1,0:T(8,128)(2,1)}, f32[64,512]{1,0:T(8,128)}, f32[64,512]{1,0:T(8,128)}) custom-call(bf16[128,2048]{1,0:T(8,128)(2,1)S(1)} %get-tuple-element.8.refs_0_, bf16[128,2048]{1,0:T(8,128)(2,1)S(1)} %get-tuple-element.9.refs_1_, f32[64,512]{1,0:T(8,128)S(1)} %get-tuple-element.10.refs_2_, ...), custom_call_target="tpu_custom_call" | custom-call | tf_op jit(solution)/shard_map/ffn_store/pallas_call | solution.py:651
